TPU v7x, 32 devices: a whole 2x2x4 slice. The times are simulated.
32 devices in a mesh: grp: 2 (over y), fs: 4 (over z), tp: 4 (over x, core).
Axes of the slice: x: 2, y: 2, z: 4, core: 2. Of those that a mesh axis runs over, the one named last changes fastest.
Arguments:
- tokens: bfloat16 [1536, 2048], P(('grp', 'fs'), 'tp'), parts along dimension 0, may hold values from -40 to 40
- routes: int32 [1536, 2], P(('grp', 'fs')), parts along dimension 0, may hold values from 0 to 3, all different within a row; in each aligned block of 192 rows (0 to 191, 192 to 383, ...) at most 112 rows name the same one
- routing_weight: float32 [1536, 2], P(('grp', 'fs')), parts along dimension 0, may hold values from 0.1 to 0.6
- norm_gain_vector: float32 [2048], P('tp'), may hold values from 0.1 to 1.9
- expert_gate: float32 [4, 512, 2048], P(None, 'fs', 'tp'), may hold values from -0.125 to 0.125
- expert_up: float32 [4, 512, 2048], P(None, 'fs', 'tp'), may hold values from -0.125 to 0.125
- expert_down: float32 [4, 512, 2048], P(None, 'fs', 'tp'), may hold values from -0.25 to 0.25
- shared_gate: float32 [512, 2048], P('fs', 'tp'), may hold values from -0.125 to 0.125
- shared_up: float32 [512, 2048], P('fs', 'tp'), may hold values from -0.125 to 0.125
- shared_down: float32 [512, 2048], P('fs', 'tp'), may hold values from -0.25 to 0.25
Outputs:
- mixed: bfloat16 [1536, 2048], P(('grp', 'fs'), 'tp'), parts along dimension 0
- gate_served: bfloat16 [8, 512, 2048], P(('grp', 'fs'), None, 'tp'), parts along dimension 0
- up_served: bfloat16 [8, 512, 2048], P(('grp', 'fs'), None, 'tp'), parts along dimension 0
- down_served: bfloat16 [8, 512, 2048], P(('grp', 'fs'), None, 'tp'), parts along dimension 0
- shared_gate_served: bfloat16 [1024, 2048], P('grp', 'tp'), parts along dimension 0
- shared_up_served: bfloat16 [1024, 2048], P('grp', 'tp'), parts along dimension 0
- shared_down_served: bfloat16 [1024, 2048], P('grp', 'tp'), parts along dimension 0
There are 2 independent parts, one for each index of `grp`. A program takes and returns all parts, laid end to end along the dimension named above; an argument that names none is the same for every part. Nothing has to cross between parts.
Inputs may be any that keep to these rules, and one draw needn't show every extreme that they name: `routes`: each row names 2 different experts. In each aligned block of 192 rows no expert is named by more than 112 rows, and in some block an expert is named by exactly 112 rows.
All inputs are finite; a program needn't handle non-finite values.
Results may differ from a plain program's by a relative error of at most 0.022.
Values may be sent and summed in bfloat16 or wider, within the bound.
A program may use at most 64 MiB of HBM per device.

v0:
```python
import functools

import jax
import jax.numpy as jnp
from jax import lax
from jax.experimental import pallas as pl
from jax.experimental.pallas import tpu as pltpu
from jax.sharding import PartitionSpec as P

norm_eps = 1e-06


def dense_rows(rows, weight):
    return lax.dot_general(
        rows, weight, (((1,), (1,)), ((), ())), preferred_element_type=jnp.float32
    )


def per_device_plain(
    tokens,
    routes,
    routing_weight,
    norm_gain_vector,
    expert_gate,
    expert_up,
    expert_down,
    shared_gate,
    shared_up,
    shared_down,
):
    tok_rows, portion_width = tokens.shape
    model_width = portion_width * lax.axis_size("tp")
    experts = expert_gate.shape[0]
    top_count = routes.shape[1]
    capacity = tok_rows * top_count * 7 // (6 * experts)
    gate_round = (expert_gate * norm_gain_vector[None, None, :]).astype(jnp.bfloat16)
    up_round = (expert_up * norm_gain_vector[None, None, :]).astype(jnp.bfloat16)
    down_round = expert_down.astype(jnp.bfloat16)
    gate_refreshed, up_new, down_new = (
        lax.all_to_all(gate_round, "fs", split_axis=0, concat_axis=1, tiled=True),
        lax.all_to_all(up_round, "fs", split_axis=0, concat_axis=1, tiled=True),
        lax.all_to_all(down_round, "fs", split_axis=0, concat_axis=1, tiled=True),
    )
    shared_g, shared_u, shared_d = (
        lax.all_gather(
            (shared_gate * norm_gain_vector[None, :]).astype(jnp.bfloat16), "fs", axis=0, tiled=True
        ),
        lax.all_gather(
            (shared_up * norm_gain_vector[None, :]).astype(jnp.bfloat16), "fs", axis=0, tiled=True
        ),
        lax.all_gather(shared_down.astype(jnp.bfloat16), "fs", axis=0, tiled=True),
    )
    values = tokens.astype(jnp.float32)
    totals = lax.psum(jnp.sum(values * values, axis=1), "tp")
    normed = (values * lax.rsqrt(totals / model_width + norm_eps)[:, None]).astype(jnp.bfloat16)
    flat_expert = routes.reshape(-1)
    onehot = (flat_expert[:, None] == jnp.arange(experts, dtype=jnp.int32)[None, :]).astype(
        jnp.int32
    )
    earlier = jnp.cumsum(onehot, axis=0) - onehot
    slot_index = jnp.sum(earlier * onehot, axis=1)
    target = (flat_expert * capacity + slot_index).reshape(tok_rows, top_count)
    places = jnp.arange(experts * capacity, dtype=jnp.int32)
    placing = jnp.sum(
        (target[:, :, None] == places[None, None, :]).astype(jnp.int32), axis=1
    ).astype(jnp.bfloat16)
    outgoing = lax.dot_general(
        placing, normed, (((0,), (0,)), ((), ())), preferred_element_type=jnp.float32
    ).astype(jnp.bfloat16)
    incoming = lax.all_to_all(
        outgoing.reshape(experts, capacity, portion_width),
        "fs",
        split_axis=0,
        concat_axis=0,
        tiled=True,
    )
    arrived = incoming.reshape(experts * capacity, portion_width)
    partials = (
        dense_rows(arrived, gate_refreshed[0]).astype(jnp.bfloat16),
        dense_rows(arrived, up_new[0]).astype(jnp.bfloat16),
        dense_rows(normed, shared_g).astype(jnp.bfloat16),
        dense_rows(normed, shared_u).astype(jnp.bfloat16),
    )
    gate_part, up_part, sgate_part, sup_part = (
        lax.psum_scatter(partials[0], "tp", scatter_dimension=1, tiled=True).astype(jnp.float32),
        lax.psum_scatter(partials[1], "tp", scatter_dimension=1, tiled=True).astype(jnp.float32),
        lax.psum_scatter(partials[2], "tp", scatter_dimension=1, tiled=True).astype(jnp.float32),
        lax.psum_scatter(partials[3], "tp", scatter_dimension=1, tiled=True).astype(jnp.float32),
    )
    hidden, shared_hidden = (
        lax.all_gather(
            (jax.nn.silu(gate_part) * up_part).astype(jnp.bfloat16), "tp", axis=1, tiled=True
        ),
        lax.all_gather(
            (jax.nn.silu(sgate_part) * sup_part).astype(jnp.bfloat16), "tp", axis=1, tiled=True
        ),
    )
    produced = jnp.dot(hidden, down_new[0], preferred_element_type=jnp.float32).astype(jnp.bfloat16)
    returned = lax.all_to_all(
        produced.reshape(experts, capacity, portion_width),
        "fs",
        split_axis=0,
        concat_axis=0,
        tiled=True,
    )
    picked = returned.reshape(experts * capacity, portion_width)[target]
    routed = jnp.sum(routing_weight[:, :, None] * picked.astype(jnp.float32), axis=1)
    shared_out = jnp.dot(shared_hidden, shared_d, preferred_element_type=jnp.float32)
    mixed = (routed + shared_out).astype(jnp.bfloat16)
    return (mixed, gate_refreshed, up_new, down_new, shared_g, shared_u, shared_d)


MESH = pl.DeviceIdType.MESH


def nearest_first(n):
    orders = [sorted(range(n), key=lambda s: (abs(s - f), s)) for f in range(n)]
    return [sum(orders[f][i] * n**f for f in range(n)) for i in range(n)]


def fused_kernel(
    n_fs, n_tp, top_count,
    tok_ref, routes_ref, weight_ref, gain_ref, eg_ref, eu_ref, ed_ref, sg_ref, su_ref, sd_ref,
    mixed_ref, wout_ref,
    wall, tokbuf, meta_ref, metabuf, ssown, ssbuf, scown, scbuf, mt, sct, part, rsbuf, hid, outf, outb, retbuf,
    tok_s, tok_r, meta_s, meta_r, ss_s, ss_r, sc_s, sc_r, rs_s, rs_r, ag_s, ag_r,
    ret_s, ret_r, we_s, we_r, ws_s, ws_r, ye_s, ye_r, ys_s, ys_r,
):
    g, f, t = lax.axis_index("grp"), lax.axis_index("fs"), lax.axis_index("tp")
    rows, width = tok_ref.shape
    experts, units = eg_ref.shape[0], eg_ref.shape[1]
    sub = rows // n_tp
    half = units // 2
    f32, bf16 = jnp.float32, jnp.bfloat16
    code = nearest_first(n_fs)

    def source(i):
        total = 0
        digits = code[i]
        picks = [(digits // n_fs**q) % n_fs for q in range(n_fs)]
        for q in range(n_fs):
            hit = 1 - jnp.minimum(1, jnp.abs(f - q))
            total = total + picks[q] * hit
        return total

    def at_fs(index):
        return (g, index, t)

    def at_tp(index):
        return (g, f, index)

    partner = (1 - g, f, t)

    def remote(src, dst, send, recv, device):
        return pltpu.make_async_remote_copy(
            src_ref=src, dst_ref=dst, send_sem=send, recv_sem=recv,
            device_id=device, device_id_type=MESH,
        )

    fs_others = [lax.rem(f + j, n_fs) for j in range(1, n_fs)]
    tp_others = [lax.rem(t + j, n_tp) for j in range(1, n_tp)]

    barrier = pltpu.get_barrier_semaphore()
    peers = [at_fs(d) for d in fs_others] + [at_tp(d) for d in tp_others] + [partner]
    for device in peers:
        pl.semaphore_signal(barrier, inc=1, device_id=device, device_id_type=MESH)
    pl.semaphore_wait(barrier, len(peers))

    def to_right(src, dst, send, recv):
        @pl.when(f < n_fs - 1)
        def _():
            remote(src, dst, send, recv, at_fs(f + 1)).start()

    def to_left(src, dst, send, recv):
        @pl.when(f > 0)
        def _():
            remote(src, dst, send, recv, at_fs(f - 1)).start()

    def onward(s, ref, send, recv):
        @pl.when((s < f) & (f < n_fs - 1))
        def _():
            remote(ref, ref, send.at[s, 0], recv.at[s], at_fs(f + 1)).start()

        @pl.when((s > f) & (f > 0))
        def _():
            remote(ref, ref, send.at[s, 1], recv.at[s], at_fs(f - 1)).start()

    def line_sends_done(refs, send, recv):
        for s in range(n_fs):
            ref = refs(s)

            @pl.when((f >= s) & (f < n_fs - 1))
            def _():
                remote(ref, ref, send.at[s, 0], recv.at[s], at_fs(f + 1)).wait_send()

            @pl.when((f <= s) & (f > 0))
            def _():
                remote(ref, ref, send.at[s, 1], recv.at[s], at_fs(f - 1)).wait_send()

    meta_ref[...] = jnp.zeros(meta_ref.shape, f32)
    meta_ref[0:top_count, 0:rows] = routes_ref[...].astype(f32)
    meta_ref[top_count : 2 * top_count, 0:rows] = weight_ref[...]
    for go, way in ((to_right, 0), (to_left, 1)):
        go(meta_ref, metabuf.at[f], meta_s.at[f, way], meta_r.at[f])
        go(tok_ref, tokbuf.at[f], tok_s.at[f, way], tok_r.at[f])

    x = tok_ref[...].astype(f32)
    sq = x * x
    high = sq.astype(bf16)
    low = (sq - high.astype(f32)).astype(bf16)
    ones = jnp.ones((8, width), bf16)
    ssown[...] = jnp.zeros(ssown.shape, f32)
    ssown[:, 0:rows] = dense_rows(ones, high) + dense_rows(ones, low)
    for d in tp_others:
        remote(ssown, ssbuf.at[t], ss_s.at[d], ss_r.at[t], at_tp(d)).start()

    gain = gain_ref[...]
    for e in range(experts):
        wall[0, e] = (eg_ref[e] * gain).astype(bf16)
        wall[1, e] = (eu_ref[e] * gain).astype(bf16)
    wall[0, experts] = (sg_ref[...] * gain).astype(bf16)
    wall[1, experts] = (su_ref[...] * gain).astype(bf16)

    def transposed(row_ref):
        return jnp.transpose(row_ref[...])[0:rows]

    def forward_block(i, tokens, meta):
        mt[i] = transposed(meta)
        names = [mt[i, :, k : k + 1] for k in range(top_count)]
        columns = []
        for m in range(2):
            weight = wall[m].reshape((experts + 1) * units, width)
            sums = dense_rows(tokens[...], weight)
            for name in names:
                chosen = jnp.zeros((rows, units), f32)
                for e in range(experts):
                    chosen = jnp.where(name == float(e), sums[:, e * units : (e + 1) * units], chosen)
                columns.append(chosen)
            columns.append(sums[:, experts * units :])
        for c, column in enumerate(columns):
            part[i, :, :, c * units : (c + 1) * units] = column.astype(bf16).reshape(n_tp, sub, units)
        for d in tp_others:
            remote(part.at[i, d], rsbuf.at[i, t], rs_s.at[i, d], rs_r.at[i, t], at_tp(d)).start()

    def hidden_block(i, scale_row):
        sct[i] = transposed(scale_row)
        own_rows = pl.ds(pl.multiple_of(t * sub, 8), sub)
        scale = sct[i, own_rows, 0:1]
        weights = mt[i, own_rows, :]
        for d in tp_others:
            remote(part.at[i, d], rsbuf.at[i, d], rs_s.at[i, d], rs_r.at[i, d], at_tp(d)).wait_recv()
        total = part[i, t].astype(f32)
        for d in tp_others:
            total = total + rsbuf[i, d].astype(f32)
        total = total * scale
        kinds = top_count + 1
        for k in range(kinds):
            gate = total[:, k * units : (k + 1) * units]
            up = total[:, (kinds + k) * units : (kinds + k + 1) * units]
            value = jax.nn.silu(gate) * up
            if k < top_count:
                value = value * weights[:, top_count + k : top_count + k + 1]
            hid[i, t, :, k * units : (k + 1) * units] = value.astype(bf16)
        for d in tp_others:
            remote(hid.at[i, t], hid.at[i, t], ag_s.at[i, d], ag_r.at[i, t], at_tp(d)).start()

    def down_block(i):
        for d in tp_others:
            remote(hid.at[i, d], hid.at[i, d], ag_s.at[i, d], ag_r.at[i, d], at_tp(d)).wait_recv()
        values = hid[i].astype(f32).reshape(rows, (top_count + 1) * units)
        names = [mt[i, :, k : k + 1] for k in range(top_count)]
        spread = []
        for e in range(experts):
            chosen = jnp.zeros((rows, units), f32)
            for k, name in enumerate(names):
                chosen = jnp.where(name == float(e), values[:, k * units : (k + 1) * units], chosen)
            spread.append(chosen.astype(bf16))
        spread.append(values[:, top_count * units :].astype(bf16))
        weight = wall[2].reshape((experts + 1) * units, width)
        return jnp.dot(jnp.concatenate(spread, axis=1), weight, preferred_element_type=f32)

    def finish_block(i):
        product = down_block(i)
        if i == 0:
            outf[...] = product
        else:
            s = source(i)
            outb[i] = product.astype(bf16)
            remote(outb.at[i], retbuf.at[f], ret_s.at[i], ret_r.at[f], at_fs(s)).start()

    def token_block(i):
        s = source(i)
        remote(metabuf.at[s], metabuf.at[s], meta_s.at[s, 0], meta_r.at[s], partner).wait_recv()
        onward(s, metabuf.at[s], meta_s, meta_r)
        remote(tokbuf.at[s], tokbuf.at[s], tok_s.at[s, 0], tok_r.at[s], partner).wait_recv()
        onward(s, tokbuf.at[s], tok_s, tok_r)

    def scale_block(i):
        s = source(i)
        remote(scown, scbuf.at[s], sc_s.at[s], sc_r.at[s], partner).wait_recv()
        return scbuf.at[s]

    for e in range(experts):
        wall[2, e] = ed_ref[e].astype(bf16)
    wall[2, experts] = sd_ref[...].astype(bf16)

    mine = pl.ds(pl.multiple_of(g * half, 16), half)
    for way, go in ((0, to_right), (1, to_left)):
        go(wall.at[:, experts, mine], wout_ref.at[1, :, f, g], ws_s.at[f, way], ws_r.at[f])

    def give_expert(i):
        d = source(i)
        remote(
            wall.at[:, d, mine], wout_ref.at[0, :, f, g], we_s.at[d], we_r.at[f], at_fs(d)
        ).start()

    def pass_shared(i):
        s = source(i)
        shared = wout_ref.at[1, :, s, g]
        remote(shared, shared, ws_s.at[s, 0], ws_r.at[s], partner).wait_recv()
        onward(s, shared, ws_s, ws_r)
        remote(shared, shared, ys_s.at[s], ys_r.at[s], partner).start()

    def pass_routed(i):
        s = source(i)
        routed = wout_ref.at[0, :, s, g]
        remote(routed, routed, we_s.at[s], we_r.at[s], partner).wait_recv()
        remote(routed, routed, ye_s.at[s], ye_r.at[s], partner).start()

    forward_block(0, tok_ref, meta_ref)
    squares = ssown[...]
    for d in tp_others:
        remote(ssown, ssbuf.at[d], ss_s.at[d], ss_r.at[d], at_tp(d)).wait_recv()
        squares = squares + ssbuf[d]
    scown[...] = lax.rsqrt(squares / (width * n_tp) + norm_eps)
    for d in fs_others:
        remote(scown, scbuf.at[f], sc_s.at[d], sc_r.at[f], at_fs(d)).start()
    for h in range(2):
        wout_ref[0, :, f, h] = wall[:, f, h * half : (h + 1) * half]
        wout_ref[1, :, f, h] = wall[:, experts, h * half : (h + 1) * half]

    for i in range(1, n_fs):
        token_block(i)
        give_expert(i)
        forward_block(i, tokbuf.at[source(i)], metabuf.at[source(i)])
        hidden_block(i - 1, scown if i == 1 else scale_block(i - 1))
        if i >= 2:
            finish_block(i - 2)
            pass_shared(i - 1)
    pass_routed(1)
    hidden_block(n_fs - 1, scale_block(n_fs - 1))
    finish_block(n_fs - 2)
    finish_block(n_fs - 1)
    pass_shared(n_fs - 1)
    for i in range(2, n_fs):
        pass_routed(i)

    total = outf[...]
    for d in fs_others:
        remote(retbuf.at[d], retbuf.at[d], ret_s.at[1], ret_r.at[d], partner).wait_recv()
        total = total + retbuf[d].astype(f32)
    mixed_ref[...] = total.astype(bf16)

    for d in fs_others:
        shared, routed = wout_ref.at[1, :, d, 1 - g], wout_ref.at[0, :, d, 1 - g]
        remote(shared, shared, ys_s.at[d], ys_r.at[d], partner).wait_recv()
        remote(routed, routed, ye_s.at[d], ye_r.at[d], partner).wait_recv()

    line_sends_done(lambda s: metabuf.at[s], meta_s, meta_r)
    line_sends_done(lambda s: tokbuf.at[s], tok_s, tok_r)
    line_sends_done(lambda s: wout_ref.at[1, :, s, g], ws_s, ws_r)
    for d in tp_others:
        remote(ssown, ssbuf.at[t], ss_s.at[d], ss_r.at[t], at_tp(d)).wait_send()
        for i in range(n_fs):
            remote(part.at[i, d], rsbuf.at[i, t], rs_s.at[i, d], rs_r.at[i, t], at_tp(d)).wait_send()
            remote(hid.at[i, t], hid.at[i, t], ag_s.at[i, d], ag_r.at[i, t], at_tp(d)).wait_send()
    for j, d in enumerate(fs_others):
        remote(scown, scbuf.at[f], sc_s.at[d], sc_r.at[f], at_fs(d)).wait_send()
        remote(outb.at[j + 1], retbuf.at[f], ret_s.at[j + 1], ret_r.at[f], at_fs(d)).wait_send()
        shared, routed = wout_ref.at[1, :, d, g], wout_ref.at[0, :, d, g]
        remote(routed, routed, we_s.at[d], we_r.at[f], at_fs(d)).wait_send()
        remote(shared, shared, ys_s.at[d], ys_r.at[d], partner).wait_send()
        remote(routed, routed, ye_s.at[d], ye_r.at[d], partner).wait_send()


def per_device_fused(
    tokens,
    routes,
    routing_weight,
    norm_gain_vector,
    expert_gate,
    expert_up,
    expert_down,
    shared_gate,
    shared_up,
    shared_down,
):
    n_fs, n_tp = lax.axis_size("fs"), lax.axis_size("tp")
    rows, width = tokens.shape
    experts, units, _ = expert_gate.shape
    top_count = routes.shape[1]
    sub, half = rows // n_tp, units // 2
    meta_rows = -(-2 * top_count // 8) * 8
    lanes = -(-rows // 128) * 128
    f32, bf16 = jnp.float32, jnp.bfloat16
    kinds = top_count + 1
    dma = pltpu.SemaphoreType.DMA
    vmem = pl.BlockSpec(memory_space=pltpu.VMEM)
    mixed, served = pl.pallas_call(
        functools.partial(fused_kernel, n_fs, n_tp, top_count),
        out_shape=(
            jax.ShapeDtypeStruct((rows, width), bf16),
            jax.ShapeDtypeStruct((2, 3, n_fs, 2, half, width), bf16),
        ),
        in_specs=[vmem] * 10,
        out_specs=(vmem, vmem),
        scratch_shapes=[
            pltpu.VMEM((3, experts + 1, units, width), bf16),
            pltpu.VMEM((n_fs, rows, width), bf16),
            pltpu.VMEM((meta_rows, lanes), f32),
            pltpu.VMEM((n_fs, meta_rows, lanes), f32),
            pltpu.VMEM((8, lanes), f32),
            pltpu.VMEM((n_tp, 8, lanes), f32),
            pltpu.VMEM((8, lanes), f32),
            pltpu.VMEM((n_fs, 8, lanes), f32),
            pltpu.VMEM((n_fs, rows, meta_rows), f32),
            pltpu.VMEM((n_fs, rows, 8), f32),
            pltpu.VMEM((n_fs, n_tp, sub, 2 * kinds * units), bf16),
            pltpu.VMEM((n_fs, n_tp, sub, 2 * kinds * units), bf16),
            pltpu.VMEM((n_fs, n_tp, sub, kinds * units), bf16),
            pltpu.VMEM((rows, width), f32),
            pltpu.VMEM((n_fs, rows, width), bf16),
            pltpu.VMEM((n_fs, rows, width), bf16),
            dma((n_fs, 2)), dma((n_fs,)),
            dma((n_fs, 2)), dma((n_fs,)),
            dma((n_tp,)), dma((n_tp,)),
            dma((n_fs,)), dma((n_fs,)),
            dma((n_fs, n_tp)), dma((n_fs, n_tp)),
            dma((n_fs, n_tp)), dma((n_fs, n_tp)),
            dma((n_fs,)), dma((n_fs,)),
            dma((n_fs,)), dma((n_fs,)),
            dma((n_fs, 2)), dma((n_fs,)),
            dma((n_fs,)), dma((n_fs,)),
            dma((n_fs,)), dma((n_fs,)),
        ],
        compiler_params=pltpu.CompilerParams(
            collective_id=0, has_side_effects=True, vmem_limit_bytes=60 * 1024 * 1024
        ),
        name="hand_over_and_layer",
    )(
        tokens, routes.T, routing_weight.T, norm_gain_vector[None, :],
        expert_gate, expert_up, expert_down, shared_gate, shared_up, shared_down,
    )
    served = served.reshape(2, 3, n_fs * units, width)
    return (
        mixed,
        served[0, 0][None], served[0, 1][None], served[0, 2][None],
        served[1, 0], served[1, 1], served[1, 2],
    )


def per_device(tokens, routes, routing_weight, norm_gain_vector, *weights):
    experts, units, width = weights[0].shape
    rows, n_fs, n_tp = tokens.shape[0], lax.axis_size("fs"), lax.axis_size("tp")
    whole_tiles = units % 128 == 0 and width % 128 == 0 and rows % (16 * n_tp) == 0
    fits = (experts + 1) * units * width <= 2**20 and n_fs <= 4 and n_tp <= 4
    chosen = per_device_plain
    if whole_tiles and fits and experts == n_fs and lax.axis_size("grp") == 2 and n_fs > 2:
        chosen = per_device_fused
    return chosen(tokens, routes, routing_weight, norm_gain_vector, *weights)


def solution(mesh):
    return jax.shard_map(
        per_device,
        mesh=mesh,
        in_specs=(
            P(("grp", "fs"), "tp"),
            P(("grp", "fs"), None),
            P(("grp", "fs"), None),
            P("tp"),
            P(None, "fs", "tp"),
            P(None, "fs", "tp"),
            P(None, "fs", "tp"),
            P("fs", "tp"),
            P("fs", "tp"),
            P("fs", "tp"),
        ),
        out_specs=(
            P(("grp", "fs"), "tp"),
            P(("grp", "fs"), None, "tp"),
            P(("grp", "fs"), None, "tp"),
            P(("grp", "fs"), None, "tp"),
            P("grp", "tp"),
            P("grp", "tp"),
            P("grp", "tp"),
        ),
        check_vma=False,
    )
```

profile of v0, /device:TPU:0, one launch (start us, length us, event | category | flops | bytes accessed | tf_op | source)
XLA Modules:
  0.0 87.7 jit_solution(13979393654172746758)
XLA Ops:
  0.6 82.8 %hand_over_and_layer.1 = (bf16[192,512]{1,0:T(8,128)(2,1)}, bf16[2,3,4,2,64,512]{5,4,3,2,1,0:T(8,128)(2,1)}) custom-call(bf16[192,512]{1,0:T(8,128)(2,1)} %tok_ref.1, s32[2,192]{1,0:T(2,128)} %bitcast.17, f32[2,192]{1,0:T(2,128)} %bitcast.18, f32[1,512]{1,0:T(1,128)} %bitcast.19, f32[4,128,512]{2,1,0:T(8,128)} %eg_ref.1, f32[4,128,512]{2,1,0:T(8,128)} %eu_ref.1, ...), custom_call_target="tpu_custom_call" | custom-call | tf_op jit(solution)/shard_map/hand_over_and_layer/pallas_call | solution.py:409
  83.5 0.0 copy-start
  83.5 3.6 %slice_bitcast_fusion = (bf16[512,512]{1,0:T(8,128)(2,1)}, bf16[512,512]{1,0:T(8,128)(2,1)}, bf16[512,512]{1,0:T(8,128)(2,1)}, bf16[1,512,512]{2,1,0:T(8,128)(2,...) fusion(bf16[2,3,512,512]{3,2,1,0:T(8,128)(2,1)} %bitcast.16), kind=kLoop, calls=%fused_computation | loop fusion | bytes 6291456 | tf_op jit(solution)/shard_map/squeeze | solution.py:458
  87.0 0.0 copy-done
  87.0 0.7 copy.18
Async XLA Ops:
  83.5 3.6 %copy-start = (bf16[192,512]{1,0:T(8,128)(2,1)S(1)}, bf16[192,512]{1,0:T(8,128)(2,1)}, u32[]{:S(2)}) copy-start(bf16[192,512]{1,0:T(8,128)(2,1)} %get-tuple-element.24) | copy-start | bytes 589828
where the time goes:
time: 87.9 us; the launch traced here: 87.7 us
  Pallas kernels  82.8 us (94%)
  local copies, waits for them, and re-layouts  4.24 us (5%)
    pallas_call x1, Pallas kernels, per_device_fused(): pl.pallas_call(functools.partial(fused_kernel, n_fs, n_tp, top_count), ou...  82.8 us
    squeeze x1, local copies, waits for them, and re-layouts, per_device_fused(): served[1, 2]  3.56 us

commit v1 on v0

--- a/solution.py
+++ b/solution.py
@@ -113,26 +113,31 @@
 MESH = pl.DeviceIdType.MESH
 
 
-def nearest_first(n):
-    orders = [sorted(range(n), key=lambda s: (abs(s - f), s)) for f in range(n)]
+def outward_first(n):
+    def key(f):
+        return lambda s: (abs(s - f), abs(2 * s - n + 1) <= abs(2 * f - n + 1), s)
+
+    orders = [sorted(range(n), key=key(f)) for f in range(n)]
     return [sum(orders[f][i] * n**f for f in range(n)) for i in range(n)]
 
 
 def fused_kernel(
     n_fs, n_tp, top_count,
-    tok_ref, routes_ref, weight_ref, gain_ref, eg_ref, eu_ref, ed_ref, sg_ref, su_ref, sd_ref,
+    tok_in, routes_in, weight_in, gain_in, eg_in, eu_in, ed_in, sg_in, su_in, sd_in,
     mixed_ref, wout_ref,
-    wall, tokbuf, meta_ref, metabuf, ssown, ssbuf, scown, scbuf, mt, sct, part, rsbuf, hid, outf, outb, retbuf,
-    tok_s, tok_r, meta_s, meta_r, ss_s, ss_r, sc_s, sc_r, rs_s, rs_r, ag_s, ag_r,
-    ret_s, ret_r, we_s, we_r, ws_s, ws_r, ye_s, ye_r, ys_s, ys_r,
+    raw, routes_ref, weight_ref, gain_ref,
+    wall, tokbuf, meta_ref, metabuf, ssown, ssbuf, scown, scbuf, mt, sct, part, rsbuf, hid, acc, outb, chain,
+    in_s, tok_s, tok_r, meta_s, meta_r, ss_s, ss_r, sc_s, sc_r, rs_s, rs_r, ag_s, ag_r,
+    ch_s, ch_r, we_s, we_r, ws_s, ws_r, yw_s, yw_r,
 ):
     g, f, t = lax.axis_index("grp"), lax.axis_index("fs"), lax.axis_index("tp")
-    rows, width = tok_ref.shape
-    experts, units = eg_ref.shape[0], eg_ref.shape[1]
+    _, _, rows, width = (n_fs, 2, 2 * tokbuf.shape[2], tokbuf.shape[3])
+    experts, units = eg_in.shape[0], eg_in.shape[1]
     sub = rows // n_tp
-    half = units // 2
+    half, mid_row = units // 2, rows // 2
     f32, bf16 = jnp.float32, jnp.bfloat16
-    code = nearest_first(n_fs)
+    code = outward_first(n_fs)
+    scope = jax.named_scope
 
     def source(i):
         total = 0
@@ -143,6 +148,9 @@
             total = total + picks[q] * hit
         return total
 
+    at_edge = (f == 0) | (f == n_fs - 1)
+    inside = (f > 0) & (f < n_fs - 1)
+
     def at_fs(index):
         return (g, index, t)
 
@@ -164,73 +172,92 @@
     peers = [at_fs(d) for d in fs_others] + [at_tp(d) for d in tp_others] + [partner]
     for device in peers:
         pl.semaphore_signal(barrier, inc=1, device_id=device, device_id_type=MESH)
-    pl.semaphore_wait(barrier, len(peers))
-
-    def to_right(src, dst, send, recv):
-        @pl.when(f < n_fs - 1)
-        def _():
-            remote(src, dst, send, recv, at_fs(f + 1)).start()
-
-    def to_left(src, dst, send, recv):
-        @pl.when(f > 0)
-        def _():
-            remote(src, dst, send, recv, at_fs(f - 1)).start()
-
-    def onward(s, ref, send, recv):
-        @pl.when((s < f) & (f < n_fs - 1))
-        def _():
-            remote(ref, ref, send.at[s, 0], recv.at[s], at_fs(f + 1)).start()
-
-        @pl.when((s > f) & (f > 0))
-        def _():
-            remote(ref, ref, send.at[s, 1], recv.at[s], at_fs(f - 1)).start()
-
-    def line_sends_done(refs, send, recv):
-        for s in range(n_fs):
-            ref = refs(s)
-
-            @pl.when((f >= s) & (f < n_fs - 1))
-            def _():
-                remote(ref, ref, send.at[s, 0], recv.at[s], at_fs(f + 1)).wait_send()
-
-            @pl.when((f <= s) & (f > 0))
-            def _():
-                remote(ref, ref, send.at[s, 1], recv.at[s], at_fs(f - 1)).wait_send()
-
+
+    loads = [pltpu.make_async_copy(tok_in.at[pl.ds(h * mid_row, mid_row)], tokbuf.at[f, h], in_s.at[h]) for h in range(2)]
+    loads.append(pltpu.make_async_copy(routes_in, routes_ref, in_s.at[2]))
+    loads.append(pltpu.make_async_copy(weight_in, weight_ref, in_s.at[3]))
+    loads.append(pltpu.make_async_copy(gain_in, gain_ref, in_s.at[4]))
+    for m, (routed, shared) in enumerate(((eg_in, sg_in), (eu_in, su_in), (ed_in, sd_in))):
+        loads.append(pltpu.make_async_copy(routed, raw.at[m, pl.ds(0, experts)], in_s.at[5 + 2 * m]))
+        loads.append(pltpu.make_async_copy(shared, raw.at[m, experts], in_s.at[6 + 2 * m]))
+    for load in loads:
+        load.start()
+    for load in loads[:4]:
+        load.wait()
     meta_ref[...] = jnp.zeros(meta_ref.shape, f32)
     meta_ref[0:top_count, 0:rows] = routes_ref[...].astype(f32)
     meta_ref[top_count : 2 * top_count, 0:rows] = weight_ref[...]
-    for go, way in ((to_right, 0), (to_left, 1)):
-        go(meta_ref, metabuf.at[f], meta_s.at[f, way], meta_r.at[f])
-        go(tok_ref, tokbuf.at[f], tok_s.at[f, way], tok_r.at[f])
-
-    x = tok_ref[...].astype(f32)
+
+    def own_tokens():
+        return tokbuf[f].reshape(rows, width)
+
+    x = own_tokens().astype(f32)
     sq = x * x
     high = sq.astype(bf16)
     low = (sq - high.astype(f32)).astype(bf16)
     ones = jnp.ones((8, width), bf16)
     ssown[...] = jnp.zeros(ssown.shape, f32)
     ssown[:, 0:rows] = dense_rows(ones, high) + dense_rows(ones, low)
+
+    with scope("barrier"):
+        pl.semaphore_wait(barrier, len(peers))
+
+    def to_right(src, dst, send, recv):
+        @pl.when(f < n_fs - 1)
+        def _():
+            remote(src, dst, send, recv, at_fs(f + 1)).start()
+
+    def to_left(src, dst, send, recv):
+        @pl.when(f > 0)
+        def _():
+            remote(src, dst, send, recv, at_fs(f - 1)).start()
+
+    def onward(s, ref, send, recv):
+        @pl.when((s < f) & (f < n_fs - 1))
+        def _():
+            remote(ref, ref, send(0), recv, at_fs(f + 1)).start()
+
+        @pl.when((s > f) & (f > 0))
+        def _():
+            remote(ref, ref, send(1), recv, at_fs(f - 1)).start()
+
+    def line_sends_done(refs, send, recv):
+        for s in range(n_fs):
+            ref = refs(s)
+
+            @pl.when((f >= s) & (f < n_fs - 1))
+            def _():
+                remote(ref, ref, send(s, 0), recv(s), at_fs(f + 1)).wait_send()
+
+            @pl.when((f <= s) & (f > 0))
+            def _():
+                remote(ref, ref, send(s, 1), recv(s), at_fs(f - 1)).wait_send()
+
+    for way, go in ((0, to_right), (1, to_left)):
+        go(meta_ref, metabuf.at[f], meta_s.at[f, way], meta_r.at[f])
+        for h in range(2):
+            go(tokbuf.at[f, h], tokbuf.at[f, h], tok_s.at[f, way, h], tok_r.at[f, h])
     for d in tp_others:
         remote(ssown, ssbuf.at[t], ss_s.at[d], ss_r.at[t], at_tp(d)).start()
 
-    gain = gain_ref[...]
-    for e in range(experts):
-        wall[0, e] = (eg_ref[e] * gain).astype(bf16)
-        wall[1, e] = (eu_ref[e] * gain).astype(bf16)
-    wall[0, experts] = (sg_ref[...] * gain).astype(bf16)
-    wall[1, experts] = (su_ref[...] * gain).astype(bf16)
+    def convert(m):
+        for load in loads[5 + 2 * m : 7 + 2 * m]:
+            load.wait()
+        for e in range(experts + 1):
+            value = raw[m, e]
+            wall[m, e] = (value * gain_ref[...] if m < 2 else value).astype(bf16)
 
     def transposed(row_ref):
         return jnp.transpose(row_ref[...])[0:rows]
 
-    def forward_block(i, tokens, meta):
+    def forward_block(i, s, meta):
         mt[i] = transposed(meta)
+        tokens = tokbuf[s].reshape(rows, width)
         names = [mt[i, :, k : k + 1] for k in range(top_count)]
         columns = []
         for m in range(2):
             weight = wall[m].reshape((experts + 1) * units, width)
-            sums = dense_rows(tokens[...], weight)
+            sums = dense_rows(tokens, weight)
             for name in names:
                 chosen = jnp.zeros((rows, units), f32)
                 for e in range(experts):
@@ -277,110 +304,237 @@
             spread.append(chosen.astype(bf16))
         spread.append(values[:, top_count * units :].astype(bf16))
         weight = wall[2].reshape((experts + 1) * units, width)
-        return jnp.dot(jnp.concatenate(spread, axis=1), weight, preferred_element_type=f32)
+        product = jnp.dot(jnp.concatenate(spread, axis=1), weight, preferred_element_type=f32)
+        acc[i] = product.reshape(2, mid_row, width)
+
+    def chain_send(i, h):
+        d = source(i)
+
+        @pl.when(d > f)
+        def _():
+            remote(outb.at[i, h], chain.at[d, h], ch_s.at[i, h], ch_r.at[d, h], at_fs(f + 1)).start()
+
+        @pl.when(d < f)
+        def _():
+            slot = d + (n_fs - d) * (1 - jnp.minimum(1, f - 1 - d))
+            remote(outb.at[i, h], chain.at[slot, h], ch_s.at[i, h], ch_r.at[slot, h], at_fs(f - 1)).start()
 
     def finish_block(i):
-        product = down_block(i)
-        if i == 0:
-            outf[...] = product
-        else:
-            s = source(i)
-            outb[i] = product.astype(bf16)
-            remote(outb.at[i], retbuf.at[f], ret_s.at[i], ret_r.at[f], at_fs(s)).start()
+        with scope(f"down{i}"):
+            down_block(i)
+        if i > 0:
+
+            @pl.when(at_edge)
+            def _():
+                for h in range(2):
+                    outb[i, h] = acc[i, h].astype(bf16)
+                    chain_send(i, h)
+
+    def chain_wait(slot, h):
+        remote(chain.at[slot, h], chain.at[slot, h], ch_s.at[1, h], ch_r.at[slot, h], partner).wait_recv()
+
+    def chain_on(i):
+        @pl.when(inside)
+        def _():
+            d = source(i)
+            for h in range(2):
+                with scope(f"chain{i}{h}"):
+                    chain_wait(d, h)
+                outb[i, h] = (acc[i, h] + chain[d, h].astype(f32)).astype(bf16)
+                chain_send(i, h)
 
     def token_block(i):
         s = source(i)
-        remote(metabuf.at[s], metabuf.at[s], meta_s.at[s, 0], meta_r.at[s], partner).wait_recv()
-        onward(s, metabuf.at[s], meta_s, meta_r)
-        remote(tokbuf.at[s], tokbuf.at[s], tok_s.at[s, 0], tok_r.at[s], partner).wait_recv()
-        onward(s, tokbuf.at[s], tok_s, tok_r)
+        with scope(f"tok{i}"):
+            remote(metabuf.at[s], metabuf.at[s], meta_s.at[s, 0], meta_r.at[s], partner).wait_recv()
+            onward(s, metabuf.at[s], lambda way: meta_s.at[s, way], meta_r.at[s])
+            for h in range(2):
+                remote(tokbuf.at[s, h], tokbuf.at[s, h], tok_s.at[s, 0, h], tok_r.at[s, h], partner).wait_recv()
+                onward(s, tokbuf.at[s, h], lambda way: tok_s.at[s, way, h], tok_r.at[s, h])
 
     def scale_block(i):
         s = source(i)
         remote(scown, scbuf.at[s], sc_s.at[s], sc_r.at[s], partner).wait_recv()
         return scbuf.at[s]
 
-    for e in range(experts):
-        wall[2, e] = ed_ref[e].astype(bf16)
-    wall[2, experts] = sd_ref[...].astype(bf16)
-
     mine = pl.ds(pl.multiple_of(g * half, 16), half)
-    for way, go in ((0, to_right), (1, to_left)):
-        go(wall.at[:, experts, mine], wout_ref.at[1, :, f, g], ws_s.at[f, way], ws_r.at[f])
+
+    def give_shared(i):
+        d = source(i)
+        for m in range(3):
+            src, dst = wall.at[m, experts, mine], wout_ref.at[1, m, f, g]
+
+            @pl.when(d == f + 1)
+            def _():
+                remote(src, dst, ws_s.at[f, 0, m], ws_r.at[f, m], at_fs(f + 1)).start()
+
+            @pl.when(d == f - 1)
+            def _():
+                remote(src, dst, ws_s.at[f, 1, m], ws_r.at[f, m], at_fs(f - 1)).start()
 
     def give_expert(i):
         d = source(i)
-        remote(
-            wall.at[:, d, mine], wout_ref.at[0, :, f, g], we_s.at[d], we_r.at[f], at_fs(d)
-        ).start()
+        for m in range(3):
+            remote(
+                wall.at[m, d, mine], wout_ref.at[0, m, f, g], we_s.at[i, m], we_r.at[f, m], at_fs(d)
+            ).start()
 
     def pass_shared(i):
         s = source(i)
-        shared = wout_ref.at[1, :, s, g]
-        remote(shared, shared, ws_s.at[s, 0], ws_r.at[s], partner).wait_recv()
-        onward(s, shared, ws_s, ws_r)
-        remote(shared, shared, ys_s.at[s], ys_r.at[s], partner).start()
+        for m in range(3):
+            ref = wout_ref.at[1, m, s, g]
+            with scope(f"S{i}{m}"):
+                remote(ref, ref, ws_s.at[s, 0, m], ws_r.at[s, m], partner).wait_recv()
+            onward(s, ref, lambda way: ws_s.at[s, way, m], ws_r.at[s, m])
+            remote(ref, ref, yw_s.at[1, s, m], yw_r.at[1, s, m], partner).start()
 
     def pass_routed(i):
         s = source(i)
-        routed = wout_ref.at[0, :, s, g]
-        remote(routed, routed, we_s.at[s], we_r.at[s], partner).wait_recv()
-        remote(routed, routed, ye_s.at[s], ye_r.at[s], partner).start()
-
-    forward_block(0, tok_ref, meta_ref)
+        for m in range(3):
+            ref = wout_ref.at[0, m, s, g]
+            with scope(f"E{i}{m}"):
+                remote(ref, ref, we_s.at[i, m], we_r.at[s, m], partner).wait_recv()
+            remote(ref, ref, yw_s.at[0, s, m], yw_r.at[0, s, m], partner).start()
+
+    loads[4].wait()
+    convert(0)
+    convert(1)
+    forward_block(0, f, meta_ref)
     squares = ssown[...]
-    for d in tp_others:
-        remote(ssown, ssbuf.at[d], ss_s.at[d], ss_r.at[d], at_tp(d)).wait_recv()
-        squares = squares + ssbuf[d]
+    with scope("sswait"):
+        for d in tp_others:
+            remote(ssown, ssbuf.at[d], ss_s.at[d], ss_r.at[d], at_tp(d)).wait_recv()
+            squares = squares + ssbuf[d]
     scown[...] = lax.rsqrt(squares / (width * n_tp) + norm_eps)
     for d in fs_others:
         remote(scown, scbuf.at[f], sc_s.at[d], sc_r.at[f], at_fs(d)).start()
+    convert(2)
+
+    @pl.when(at_edge)
+    def _():
+        give_shared(1)
+        for i in range(1, n_fs):
+            give_expert(i)
+
     for h in range(2):
         wout_ref[0, :, f, h] = wall[:, f, h * half : (h + 1) * half]
         wout_ref[1, :, f, h] = wall[:, experts, h * half : (h + 1) * half]
 
-    for i in range(1, n_fs):
+    def arrive(i):
         token_block(i)
-        give_expert(i)
-        forward_block(i, tokbuf.at[source(i)], metabuf.at[source(i)])
-        hidden_block(i - 1, scown if i == 1 else scale_block(i - 1))
-        if i >= 2:
-            finish_block(i - 2)
-            pass_shared(i - 1)
+
+        if i == 1:
+
+            @pl.when(inside)
+            def _():
+                give_shared(2)
+                give_expert(2)
+
+        if i == n_fs - 1:
+
+            @pl.when(inside)
+            def _():
+                give_shared(1)
+                give_expert(1)
+
+        with scope(f"fwd{i}"):
+            forward_block(i, source(i), metabuf.at[source(i)])
+
+    def hide(i):
+        with scope(f"hid{i}"):
+            hidden_block(i, scown if i == 0 else scale_block(i))
+
+    arrive(1)
+    arrive(2)
+    hide(0)
+    arrive(3)
+    hide(1)
+    hide(2)
+    finish_block(0)
+    finish_block(1)
+    pass_shared(1)
+
+    @pl.when(inside)
+    def _():
+        give_expert(n_fs - 1)
+
+    hide(3)
+    finish_block(2)
+
+    @pl.when(inside)
+    def _():
+        pass_shared(2)
+
+    finish_block(3)
     pass_routed(1)
-    hidden_block(n_fs - 1, scale_block(n_fs - 1))
-    finish_block(n_fs - 2)
-    finish_block(n_fs - 1)
-    pass_shared(n_fs - 1)
-    for i in range(2, n_fs):
-        pass_routed(i)
-
-    total = outf[...]
-    for d in fs_others:
-        remote(retbuf.at[d], retbuf.at[d], ret_s.at[1], ret_r.at[d], partner).wait_recv()
-        total = total + retbuf[d].astype(f32)
-    mixed_ref[...] = total.astype(bf16)
-
-    for d in fs_others:
-        shared, routed = wout_ref.at[1, :, d, 1 - g], wout_ref.at[0, :, d, 1 - g]
-        remote(shared, shared, ys_s.at[d], ys_r.at[d], partner).wait_recv()
-        remote(routed, routed, ye_s.at[d], ye_r.at[d], partner).wait_recv()
-
-    line_sends_done(lambda s: metabuf.at[s], meta_s, meta_r)
-    line_sends_done(lambda s: tokbuf.at[s], tok_s, tok_r)
-    line_sends_done(lambda s: wout_ref.at[1, :, s, g], ws_s, ws_r)
-    for d in tp_others:
-        remote(ssown, ssbuf.at[t], ss_s.at[d], ss_r.at[t], at_tp(d)).wait_send()
-        for i in range(n_fs):
-            remote(part.at[i, d], rsbuf.at[i, t], rs_s.at[i, d], rs_r.at[i, t], at_tp(d)).wait_send()
-            remote(hid.at[i, t], hid.at[i, t], ag_s.at[i, d], ag_r.at[i, t], at_tp(d)).wait_send()
-    for j, d in enumerate(fs_others):
-        remote(scown, scbuf.at[f], sc_s.at[d], sc_r.at[f], at_fs(d)).wait_send()
-        remote(outb.at[j + 1], retbuf.at[f], ret_s.at[j + 1], ret_r.at[f], at_fs(d)).wait_send()
-        shared, routed = wout_ref.at[1, :, d, g], wout_ref.at[0, :, d, g]
-        remote(routed, routed, we_s.at[d], we_r.at[f], at_fs(d)).wait_send()
-        remote(shared, shared, ys_s.at[d], ys_r.at[d], partner).wait_send()
-        remote(routed, routed, ye_s.at[d], ye_r.at[d], partner).wait_send()
+
+    @pl.when(at_edge)
+    def _():
+        pass_shared(2)
+
+    pass_routed(2)
+    pass_shared(3)
+    chain_on(2)
+    pass_routed(3)
+    chain_on(3)
+    chain_on(1)
+
+    for h in range(2):
+        with scope(f"last{h}"):
+
+            @pl.when(f > 0)
+            def _():
+                chain_wait(f, h)
+                acc[0, h] = acc[0, h] + chain[f, h].astype(f32)
+
+            @pl.when(f < n_fs - 1)
+            def _():
+                chain_wait(n_fs, h)
+                acc[0, h] = acc[0, h] + chain[n_fs, h].astype(f32)
+
+        mixed_ref[h * mid_row : (h + 1) * mid_row] = acc[0, h].astype(bf16)
+
+    with scope("ywait"):
+        for d in fs_others:
+            for kind in range(2):
+                for m in range(3):
+                    ref = wout_ref.at[kind, m, d, 1 - g]
+                    remote(ref, ref, yw_s.at[kind, d, m], yw_r.at[kind, d, m], partner).wait_recv()
+
+    with scope("drain"):
+        line_sends_done(lambda s: metabuf.at[s], lambda s, way: meta_s.at[s, way], lambda s: meta_r.at[s])
+        for h in range(2):
+            line_sends_done(lambda s: tokbuf.at[s, h], lambda s, way: tok_s.at[s, way, h], lambda s: tok_r.at[s, h])
+        for m in range(3):
+            line_sends_done(
+                lambda s: wout_ref.at[1, m, s, g], lambda s, way: ws_s.at[s, way, m], lambda s: ws_r.at[s, m]
+            )
+        for d in tp_others:
+            remote(ssown, ssbuf.at[t], ss_s.at[d], ss_r.at[t], at_tp(d)).wait_send()
+            for i in range(n_fs):
+                remote(part.at[i, d], rsbuf.at[i, t], rs_s.at[i, d], rs_r.at[i, t], at_tp(d)).wait_send()
+                remote(hid.at[i, t], hid.at[i, t], ag_s.at[i, d], ag_r.at[i, t], at_tp(d)).wait_send()
+        for d in fs_others:
+            remote(scown, scbuf.at[f], sc_s.at[d], sc_r.at[f], at_fs(d)).wait_send()
+        for i in range(1, n_fs):
+            s = source(i)
+            for h in range(2):
+                remote(outb.at[i, h], chain.at[f, h], ch_s.at[i, h], ch_r.at[f, h], partner).wait_send()
+            for m in range(3):
+                routed, shared = wout_ref.at[0, m, s, g], wout_ref.at[1, m, s, g]
+                remote(routed, routed, we_s.at[i, m], we_r.at[f, m], partner).wait_send()
+                remote(routed, routed, yw_s.at[0, s, m], yw_r.at[0, s, m], partner).wait_send()
+                remote(shared, shared, yw_s.at[1, s, m], yw_r.at[1, s, m], partner).wait_send()
+
+
+def put_out(mixed_ref, served_ref, *rest):
+    outs, sems = rest[:-1], rest[-1]
+    copies = [pltpu.make_async_copy(served_ref.at[i], outs[1 + i], sems.at[1 + i]) for i in range(len(outs) - 1)]
+    copies.append(pltpu.make_async_copy(mixed_ref, outs[0], sems.at[0]))
+    for copy in copies:
+        copy.start()
+    for copy in copies:
+        copy.wait()
 
 
 def per_device_fused(
@@ -406,17 +560,22 @@
     kinds = top_count + 1
     dma = pltpu.SemaphoreType.DMA
     vmem = pl.BlockSpec(memory_space=pltpu.VMEM)
+    hbm = pl.BlockSpec(memory_space=pltpu.HBM)
     mixed, served = pl.pallas_call(
         functools.partial(fused_kernel, n_fs, n_tp, top_count),
         out_shape=(
-            jax.ShapeDtypeStruct((rows, width), bf16),
-            jax.ShapeDtypeStruct((2, 3, n_fs, 2, half, width), bf16),
-        ),
-        in_specs=[vmem] * 10,
+            pltpu.VMEM((rows, width), bf16),
+            pltpu.VMEM((2, 3, n_fs, 2, half, width), bf16),
+        ),
+        in_specs=[hbm] * 10,
         out_specs=(vmem, vmem),
         scratch_shapes=[
+            pltpu.VMEM((3, experts + 1, units, width), f32),
+            pltpu.VMEM((top_count, rows), jnp.int32),
+            pltpu.VMEM((top_count, rows), f32),
+            pltpu.VMEM((1, width), f32),
             pltpu.VMEM((3, experts + 1, units, width), bf16),
-            pltpu.VMEM((n_fs, rows, width), bf16),
+            pltpu.VMEM((n_fs, 2, rows // 2, width), bf16),
             pltpu.VMEM((meta_rows, lanes), f32),
             pltpu.VMEM((n_fs, meta_rows, lanes), f32),
             pltpu.VMEM((8, lanes), f32),
@@ -428,44 +587,55 @@
             pltpu.VMEM((n_fs, n_tp, sub, 2 * kinds * units), bf16),
             pltpu.VMEM((n_fs, n_tp, sub, 2 * kinds * units), bf16),
             pltpu.VMEM((n_fs, n_tp, sub, kinds * units), bf16),
-            pltpu.VMEM((rows, width), f32),
-            pltpu.VMEM((n_fs, rows, width), bf16),
-            pltpu.VMEM((n_fs, rows, width), bf16),
-            dma((n_fs, 2)), dma((n_fs,)),
+            pltpu.VMEM((n_fs, 2, rows // 2, width), f32),
+            pltpu.VMEM((n_fs, 2, rows // 2, width), bf16),
+            pltpu.VMEM((n_fs + 1, 2, rows // 2, width), bf16),
+            dma((11,)),
+            dma((n_fs, 2, 2)), dma((n_fs, 2)),
             dma((n_fs, 2)), dma((n_fs,)),
             dma((n_tp,)), dma((n_tp,)),
             dma((n_fs,)), dma((n_fs,)),
             dma((n_fs, n_tp)), dma((n_fs, n_tp)),
             dma((n_fs, n_tp)), dma((n_fs, n_tp)),
-            dma((n_fs,)), dma((n_fs,)),
-            dma((n_fs,)), dma((n_fs,)),
-            dma((n_fs, 2)), dma((n_fs,)),
-            dma((n_fs,)), dma((n_fs,)),
-            dma((n_fs,)), dma((n_fs,)),
+            dma((n_fs, 2)), dma((n_fs + 1, 2)),
+            dma((n_fs, 3)), dma((n_fs, 3)),
+            dma((n_fs, 2, 3)), dma((n_fs, 3)),
+            dma((2, n_fs, 3)), dma((2, n_fs, 3)),
         ],
         compiler_params=pltpu.CompilerParams(
-            collective_id=0, has_side_effects=True, vmem_limit_bytes=60 * 1024 * 1024
+            collective_id=0, has_side_effects=True, vmem_limit_bytes=40 * 1024 * 1024
         ),
         name="hand_over_and_layer",
-    )(
-        tokens, routes.T, routing_weight.T, norm_gain_vector[None, :],
-        expert_gate, expert_up, expert_down, shared_gate, shared_up, shared_down,
-    )
-    served = served.reshape(2, 3, n_fs * units, width)
-    return (
-        mixed,
-        served[0, 0][None], served[0, 1][None], served[0, 2][None],
-        served[1, 0], served[1, 1], served[1, 2],
-    )
+    )(*[
+        pltpu.with_memory_space_constraint(value, pltpu.HBM)
+        for value in (
+            tokens, routes.T, routing_weight.T, norm_gain_vector[None, :],
+            expert_gate, expert_up, expert_down, shared_gate, shared_up, shared_down,
+        )
+    ])
+    units_all = n_fs * units
+    outs = pl.pallas_call(
+        put_out,
+        out_shape=(
+            jax.ShapeDtypeStruct((rows, width), bf16),
+            *[jax.ShapeDtypeStruct((units_all, width), bf16)] * 6,
+        ),
+        in_specs=[vmem] * 2,
+        out_specs=(hbm,) * 7,
+        scratch_shapes=[dma((7,))],
+        compiler_params=pltpu.CompilerParams(vmem_limit_bytes=8 * 1024 * 1024),
+        name="put_out",
+    )(mixed, served.reshape(6, units_all, width))
+    return (outs[0], outs[1][None], outs[2][None], outs[3][None], *outs[4:])
 
 
 def per_device(tokens, routes, routing_weight, norm_gain_vector, *weights):
     experts, units, width = weights[0].shape
     rows, n_fs, n_tp = tokens.shape[0], lax.axis_size("fs"), lax.axis_size("tp")
     whole_tiles = units % 128 == 0 and width % 128 == 0 and rows % (16 * n_tp) == 0
-    fits = (experts + 1) * units * width <= 2**20 and n_fs <= 4 and n_tp <= 4
+    fits = (experts + 1) * units * width <= 2**20 and n_fs == 4 and n_tp <= 4
     chosen = per_device_plain
-    if whole_tiles and fits and experts == n_fs and lax.axis_size("grp") == 2 and n_fs > 2:
+    if whole_tiles and fits and experts == n_fs and lax.axis_size("grp") == 2:
         chosen = per_device_fused
     return chosen(tokens, routes, routing_weight, norm_gain_vector, *weights)
 

time: 87.9 us -> 65.6 us (0.75)
  Pallas kernels: 82.8 us -> 64.8 us
  local copies, waits for them, and re-layouts: 4.24 us -> 0 us
    pallas_call x1, Pallas kernels: 82.8 us -> 63.1 us  [per_device_fused(): pl.pallas_call(functools.partial(fused_kernel, n_fs, n_tp, top_count), ou...]
    squeeze x1 -> x0, local copies, waits for them, and re-layouts: 3.56 us -> none  [per_device_fused(): served[1, 2]]
    pallas_call x0 -> x1, Pallas kernels: none -> 1.78 us  [per_device_fused(): pl.pallas_call(put_out, out_shape=(jax.ShapeDtypeStruct((rows, width), bf...]
where the time goes in v1:
time: 65.6 us; the launch traced here: 65.5 us
  Pallas kernels  64.8 us (99%)
    pallas_call x1, Pallas kernels, per_device_fused(): pl.pallas_call(functools.partial(fused_kernel, n_fs, n_tp, top_count), ou...  63.1 us
    pallas_call x1, Pallas kernels, per_device_fused(): pl.pallas_call(put_out, out_shape=(jax.ShapeDtypeStruct((rows, width), bf...  1.78 us

profile of v1, /device:TPU:0, one launch (start us, length us, event | category | flops | bytes accessed | tf_op | source)
XLA Modules:
  0.0 65.5 jit_solution(12128995281961557412)
XLA Ops:
  0.6 63.1 %hand_over_and_layer.1 = (bf16[192,512]{1,0:T(8,128)(2,1)S(1)}, bf16[2,3,4,2,64,512]{5,4,3,2,1,0:T(8,128)(2,1)S(1)}) custom-call(bf16[192,512]{1,0:T(8,128)(2,1)} %tok_in.1, s32[2,192]{1,0:T(2,128)} %bitcast.8, f32[2,192]{1,0:T(2,128)} %bitcast.9, f32[1,512]{1,0:T(1,128)} %bitcast.10, f32[4,128,512]{2,1,0:T(8,128)} %eg_in.1, f32[4,128,512]{2,1,0:T(8,128)} %eu_in.1, ...), custom_call_target="tpu_custom_call" | custom-call | tf_op jit(solution)/shard_map/hand_over_and_layer/pallas_call | solution.py:564
  63.7 1.8 %put_out.1 = (bf16[192,512]{1,0:T(8,128)(2,1)}, bf16[512,512]{1,0:T(8,128)(2,1)}, bf16[512,512]{1,0:T(8,128)(2,1)}, bf16[512,512]{1,0:T(8,128)(2,1)}, bf16[512,5...) custom-call(bf16[192,512]{1,0:T(8,128)(2,1)S(1)} %get-tuple-element.16.mixed_ref, ...), custom_call_target="tpu_custom_call" | custom-call | tf_op jit(solution)/shard_map/put_out/pallas_call | solution.py:617

commit v2 on v1

v2 whole, which is shorter than its diff:
```python
import functools

import jax
import jax.numpy as jnp
from jax import lax
from jax.experimental import pallas as pl
from jax.experimental.pallas import tpu as pltpu
from jax.sharding import PartitionSpec as P

norm_eps = 1e-06


def dense_rows(rows, weight):
    return lax.dot_general(
        rows, weight, (((1,), (1,)), ((), ())), preferred_element_type=jnp.float32
    )


def per_device_plain(
    tokens,
    routes,
    routing_weight,
    norm_gain_vector,
    expert_gate,
    expert_up,
    expert_down,
    shared_gate,
    shared_up,
    shared_down,
):
    tok_rows, portion_width = tokens.shape
    model_width = portion_width * lax.axis_size("tp")
    experts = expert_gate.shape[0]
    top_count = routes.shape[1]
    capacity = tok_rows * top_count * 7 // (6 * experts)
    gate_round = (expert_gate * norm_gain_vector[None, None, :]).astype(jnp.bfloat16)
    up_round = (expert_up * norm_gain_vector[None, None, :]).astype(jnp.bfloat16)
    down_round = expert_down.astype(jnp.bfloat16)
    gate_refreshed, up_new, down_new = (
        lax.all_to_all(gate_round, "fs", split_axis=0, concat_axis=1, tiled=True),
        lax.all_to_all(up_round, "fs", split_axis=0, concat_axis=1, tiled=True),
        lax.all_to_all(down_round, "fs", split_axis=0, concat_axis=1, tiled=True),
    )
    shared_g, shared_u, shared_d = (
        lax.all_gather(
            (shared_gate * norm_gain_vector[None, :]).astype(jnp.bfloat16), "fs", axis=0, tiled=True
        ),
        lax.all_gather(
            (shared_up * norm_gain_vector[None, :]).astype(jnp.bfloat16), "fs", axis=0, tiled=True
        ),
        lax.all_gather(shared_down.astype(jnp.bfloat16), "fs", axis=0, tiled=True),
    )
    values = tokens.astype(jnp.float32)
    totals = lax.psum(jnp.sum(values * values, axis=1), "tp")
    normed = (values * lax.rsqrt(totals / model_width + norm_eps)[:, None]).astype(jnp.bfloat16)
    flat_expert = routes.reshape(-1)
    onehot = (flat_expert[:, None] == jnp.arange(experts, dtype=jnp.int32)[None, :]).astype(
        jnp.int32
    )
    earlier = jnp.cumsum(onehot, axis=0) - onehot
    slot_index = jnp.sum(earlier * onehot, axis=1)
    target = (flat_expert * capacity + slot_index).reshape(tok_rows, top_count)
    places = jnp.arange(experts * capacity, dtype=jnp.int32)
    placing = jnp.sum(
        (target[:, :, None] == places[None, None, :]).astype(jnp.int32), axis=1
    ).astype(jnp.bfloat16)
    outgoing = lax.dot_general(
        placing, normed, (((0,), (0,)), ((), ())), preferred_element_type=jnp.float32
    ).astype(jnp.bfloat16)
    incoming = lax.all_to_all(
        outgoing.reshape(experts, capacity, portion_width),
        "fs",
        split_axis=0,
        concat_axis=0,
        tiled=True,
    )
    arrived = incoming.reshape(experts * capacity, portion_width)
    partials = (
        dense_rows(arrived, gate_refreshed[0]).astype(jnp.bfloat16),
        dense_rows(arrived, up_new[0]).astype(jnp.bfloat16),
        dense_rows(normed, shared_g).astype(jnp.bfloat16),
        dense_rows(normed, shared_u).astype(jnp.bfloat16),
    )
    gate_part, up_part, sgate_part, sup_part = (
        lax.psum_scatter(partials[0], "tp", scatter_dimension=1, tiled=True).astype(jnp.float32),
        lax.psum_scatter(partials[1], "tp", scatter_dimension=1, tiled=True).astype(jnp.float32),
        lax.psum_scatter(partials[2], "tp", scatter_dimension=1, tiled=True).astype(jnp.float32),
        lax.psum_scatter(partials[3], "tp", scatter_dimension=1, tiled=True).astype(jnp.float32),
    )
    hidden, shared_hidden = (
        lax.all_gather(
            (jax.nn.silu(gate_part) * up_part).astype(jnp.bfloat16), "tp", axis=1, tiled=True
        ),
        lax.all_gather(
            (jax.nn.silu(sgate_part) * sup_part).astype(jnp.bfloat16), "tp", axis=1, tiled=True
        ),
    )
    produced = jnp.dot(hidden, down_new[0], preferred_element_type=jnp.float32).astype(jnp.bfloat16)
    returned = lax.all_to_all(
        produced.reshape(experts, capacity, portion_width),
        "fs",
        split_axis=0,
        concat_axis=0,
        tiled=True,
    )
    picked = returned.reshape(experts * capacity, portion_width)[target]
    routed = jnp.sum(routing_weight[:, :, None] * picked.astype(jnp.float32), axis=1)
    shared_out = jnp.dot(shared_hidden, shared_d, preferred_element_type=jnp.float32)
    mixed = (routed + shared_out).astype(jnp.bfloat16)
    return (mixed, gate_refreshed, up_new, down_new, shared_g, shared_u, shared_d)


MESH = pl.DeviceIdType.MESH


def outward_first(n):
    def key(f):
        return lambda s: (abs(s - f), abs(2 * s - n + 1) <= abs(2 * f - n + 1), s)

    orders = [sorted(range(n), key=key(f)) for f in range(n)]
    return [sum(orders[f][i] * n**f for f in range(n)) for i in range(n)]


def fused_kernel(
    n_fs, n_tp, top_count,
    tok_in, routes_in, weight_in, gain_in, eg_in, eu_in, ed_in, sg_in, su_in, sd_in,
    mixed_ref, wout_ref,
    raw, routes_ref, weight_ref, gain_ref,
    wall, tokbuf, meta_ref, metabuf, ssown, ssbuf, scown, scbuf, mt, sct, part, rsbuf, hid, acc, outb, chain,
    in_s, tok_s, tok_r, meta_s, meta_r, ss_s, ss_r, sc_s, sc_r, rs_s, rs_r, ag_s, ag_r,
    ch_s, ch_r, we_s, we_r, ws_s, ws_r, yw_s, yw_r,
):
    g, f, t = lax.axis_index("grp"), lax.axis_index("fs"), lax.axis_index("tp")
    rows, width = tokbuf.shape[1:]
    experts, units = eg_in.shape[0], eg_in.shape[1]
    sub = rows // n_tp
    half = units // 2
    f32, bf16 = jnp.float32, jnp.bfloat16
    code = outward_first(n_fs)
    scope = jax.named_scope
    parts = [pl.ds(h * (rows // 2), rows // 2) for h in range(2)]
    three = pl.ds(0, n_tp - 1)

    def source(i):
        total = 0
        digits = code[i]
        picks = [(digits // n_fs**q) % n_fs for q in range(n_fs)]
        for q in range(n_fs):
            hit = 1 - jnp.minimum(1, jnp.abs(f - q))
            total = total + picks[q] * hit
        return total

    at_edge = (f == 0) | (f == n_fs - 1)
    inside = (f > 0) & (f < n_fs - 1)

    def at_fs(index):
        return (g, index, t)

    def at_tp(index):
        return (g, f, index)

    partner = (1 - g, f, t)

    def remote(src, dst, send, recv, device):
        return pltpu.make_async_remote_copy(
            src_ref=src, dst_ref=dst, send_sem=send, recv_sem=recv,
            device_id=device, device_id_type=MESH,
        )

    def sent(ref, send):
        remote(ref, ref, send, send, partner).wait_send()

    def landed(ref, recv):
        remote(ref, ref, recv, recv, partner).wait_recv()

    fs_others = [lax.rem(f + j, n_fs) for j in range(1, n_fs)]
    tp_others = [lax.rem(t + j, n_tp) for j in range(1, n_tp)]

    barrier = pltpu.get_barrier_semaphore()
    peers = [at_fs(d) for d in fs_others] + [at_tp(d) for d in tp_others] + [partner]
    for device in peers:
        pl.semaphore_signal(barrier, inc=1, device_id=device, device_id_type=MESH)

    small = [
        pltpu.make_async_copy(tok_in, tokbuf.at[f], in_s.at[0]),
        pltpu.make_async_copy(routes_in, routes_ref, in_s.at[1]),
        pltpu.make_async_copy(weight_in, weight_ref, in_s.at[2]),
        pltpu.make_async_copy(gain_in, gain_ref, in_s.at[3]),
    ]
    for load in small:
        load.start()
    for m, (routed, shared) in enumerate(((eg_in, sg_in), (eu_in, su_in), (ed_in, sd_in))):
        pltpu.make_async_copy(routed, raw.at[m, pl.ds(0, experts)], in_s.at[4 + m]).start()
        pltpu.make_async_copy(shared, raw.at[m, experts], in_s.at[4 + m]).start()
    for load in small:
        load.wait()
    meta_ref[...] = jnp.zeros(meta_ref.shape, f32)
    meta_ref[0:top_count, 0:rows] = routes_ref[...].astype(f32)
    meta_ref[top_count : 2 * top_count, 0:rows] = weight_ref[...]

    x = tokbuf[f].astype(f32)
    sq = x * x
    high = sq.astype(bf16)
    low = (sq - high.astype(f32)).astype(bf16)
    ones = jnp.ones((8, width), bf16)
    ssown[...] = jnp.zeros(ssown.shape, f32)
    ssown[:, 0:rows] = dense_rows(ones, high) + dense_rows(ones, low)

    with scope("barrier"):
        pl.semaphore_wait(barrier, len(peers))

    def convert(m):
        pltpu.make_async_copy(raw.at[m], raw.at[m], in_s.at[4 + m]).wait()
        for e in range(experts + 1):
            value = raw[m, e]
            wall[m, e] = (value * gain_ref[...] if m < 2 else value).astype(bf16)

    def transposed(row_ref):
        return jnp.transpose(row_ref[...])[0:rows]

    def forward_block(i):
        s = source(i)
        with scope(f"fwd{i}"):
            mt[i] = transposed(meta_ref if i == 0 else metabuf.at[s])
            tokens = tokbuf[s]
            names = [mt[i, :, k : k + 1] for k in range(top_count)]
            columns = []
            for m in range(2):
                weight = wall[m].reshape((experts + 1) * units, width)
                sums = dense_rows(tokens, weight)
                for name in names:
                    chosen = jnp.zeros((rows, units), f32)
                    for e in range(experts):
                        chosen = jnp.where(name == float(e), sums[:, e * units : (e + 1) * units], chosen)
                    columns.append(chosen)
                columns.append(sums[:, experts * units :])
            for c, column in enumerate(columns):
                part[i, :, :, c * units : (c + 1) * units] = column.astype(bf16).reshape(n_tp, sub, units)
            for d in tp_others:
                remote(part.at[i, d], rsbuf.at[i, t], rs_s.at[0], rs_r.at[i], at_tp(d)).start()

    def hidden_block(i):
        s = source(i)
        with scope(f"hid{i}"):
            if i > 0:
                landed(scbuf.at[s], sc_r.at[s])
            sct[i] = transposed(scown if i == 0 else scbuf.at[s])
            own_rows = pl.ds(pl.multiple_of(t * sub, 8), sub)
            scale = sct[i, own_rows, 0:1]
            weights = mt[i, own_rows, :]
            landed(rsbuf.at[i, three], rs_r.at[i])
            total = part[i, t].astype(f32)
            for d in tp_others:
                total = total + rsbuf[i, d].astype(f32)
            total = total * scale
            kinds = top_count + 1
            for k in range(kinds):
                gate = total[:, k * units : (k + 1) * units]
                up = total[:, (kinds + k) * units : (kinds + k + 1) * units]
                value = jax.nn.silu(gate) * up
                if k < top_count:
                    value = value * weights[:, top_count + k : top_count + k + 1]
                hid[i, t, :, k * units : (k + 1) * units] = value.astype(bf16)
            for d in tp_others:
                remote(hid.at[i, t], hid.at[i, t], ag_s.at[0], ag_r.at[i], at_tp(d)).start()

    def down_block(i):
        with scope(f"down{i}"):
            landed(hid.at[i, three], ag_r.at[i])
            values = hid[i].astype(f32).reshape(rows, (top_count + 1) * units)
            names = [mt[i, :, k : k + 1] for k in range(top_count)]
            spread = []
            for e in range(experts):
                chosen = jnp.zeros((rows, units), f32)
                for k, name in enumerate(names):
                    chosen = jnp.where(name == float(e), values[:, k * units : (k + 1) * units], chosen)
                spread.append(chosen.astype(bf16))
            spread.append(values[:, top_count * units :].astype(bf16))
            weight = wall[2].reshape((experts + 1) * units, width)
            acc[i] = jnp.dot(jnp.concatenate(spread, axis=1), weight, preferred_element_type=f32)

    def chain_send(i, h, hop, last):
        d = source(i)
        slot = d
        if last:
            slot = d + (n_fs - d) * jnp.minimum(1, jnp.maximum(0, f - d))
        remote(
            outb.at[i, parts[h]], chain.at[slot, parts[h]], ch_s.at[0], ch_r.at[slot, h], at_fs(source(hop))
        ).start()

    def chain_start(i):
        for h in range(2):
            outb[i, parts[h]] = acc[i, parts[h]].astype(bf16)
            chain_send(i, h, 1, i == 1)

    def chain_on(i, h):
        d = source(i)
        with scope(f"chain{i}{h}"):
            landed(chain.at[d, parts[h]], ch_r.at[d, h])
        outb[i, parts[h]] = (acc[i, parts[h]] + chain[d, parts[h]].astype(f32)).astype(bf16)
        chain_send(i, h, min(i, 2), i < 3)

    def chain_end(slot, h):
        with scope(f"last{h}"):
            landed(chain.at[slot, parts[h]], ch_r.at[slot, h])
        acc[0, parts[h]] = acc[0, parts[h]] + chain[slot, parts[h]].astype(f32)

    def tokens_to(hop, s, h):
        ref = tokbuf.at[s, parts[h]]
        remote(ref, ref, tok_s.at[0], tok_r.at[s, h], at_fs(source(hop))).start()

    def meta_to(hop, s):
        remote(
            meta_ref if s is f else metabuf.at[s], metabuf.at[s], meta_s.at[0], meta_r.at[s], at_fs(source(hop))
        ).start()

    def take_tokens(i, h, hop=None):
        s = source(i)
        with scope(f"tok{i}{h}"):
            if h == 0:
                landed(metabuf.at[s], meta_r.at[s])
                if hop:
                    meta_to(hop, s)
            landed(tokbuf.at[s, parts[h]], tok_r.at[s, h])
            if hop:
                tokens_to(hop, s, h)

    mine = pl.ds(pl.multiple_of(g * half, 16), half)

    def give_shared(hop, pieces=(0, 1, 2)):
        for m in pieces:
            remote(
                wall.at[m, experts, mine], wout_ref.at[1, m, f, g], ws_s.at[0], ws_r.at[f, m], at_fs(source(hop))
            ).start()

    def give_expert(i):
        d = source(i)
        for m in range(3):
            remote(wall.at[m, d, mine], wout_ref.at[0, m, f, g], we_s.at[0], we_r.at[f, m], at_fs(d)).start()

    def pass_shared(i, m, hop=None):
        s = source(i)
        ref = wout_ref.at[1, m, s, g]
        with scope(f"S{i}{m}"):
            landed(ref, ws_r.at[s, m])
        if hop:
            remote(ref, ref, ws_s.at[0], ws_r.at[s, m], at_fs(source(hop))).start()
        remote(ref, ref, yw_s.at[0], yw_r.at[0], partner).start()

    def pass_routed(i, m):
        s = source(i)
        ref = wout_ref.at[0, m, s, g]
        with scope(f"E{i}{m}"):
            landed(ref, we_r.at[s, m])
        remote(ref, ref, yw_s.at[0], yw_r.at[0], partner).start()

    def start_up():
        for d in tp_others:
            remote(ssown, ssbuf.at[t], ss_s.at[0], ss_r.at[0], at_tp(d)).start()
        convert(0)
        convert(1)
        forward_block(0)
        squares = ssown[...]
        with scope("sswait"):
            landed(ssbuf.at[three], ss_r.at[0])
        for d in tp_others:
            squares = squares + ssbuf[d]
        scown[...] = lax.rsqrt(squares / (width * n_tp) + norm_eps)
        for d in fs_others:
            remote(scown, scbuf.at[f], sc_s.at[0], sc_r.at[f], at_fs(d)).start()
        convert(2)

    def keep_own():
        for h in range(2):
            wout_ref[0, :, f, h] = wall[:, f, h * half : (h + 1) * half]
            wout_ref[1, :, f, h] = wall[:, experts, h * half : (h + 1) * half]

    def finish():
        mixed_ref[...] = acc[0].astype(bf16)

    @pl.when(at_edge)
    def _():
        meta_to(1, f)
        for h in range(2):
            tokens_to(1, f, h)
        start_up()
        give_shared(1)
        for i in range(1, n_fs):
            give_expert(i)
        keep_own()
        take_tokens(1, 0)
        take_tokens(1, 1)
        forward_block(1)
        hidden_block(0)
        take_tokens(2, 0)
        take_tokens(2, 1)
        forward_block(2)
        hidden_block(1)
        down_block(0)
        pass_shared(1, 0)
        take_tokens(3, 0)
        take_tokens(3, 1)
        forward_block(3)
        hidden_block(2)
        down_block(1)
        chain_start(1)
        pass_shared(1, 1)
        pass_routed(3, 0)
        hidden_block(3)
        pass_routed(3, 1)
        pass_routed(3, 2)
        down_block(2)
        pass_shared(1, 2)
        down_block(3)
        chain_start(3)
        chain_start(2)
        for m in range(3):
            pass_routed(1, m)
        pass_shared(2, 0)
        pass_shared(2, 1)
        for m in range(3):
            pass_routed(2, m)
        pass_shared(2, 2)
        for m in range(3):
            pass_shared(3, m)
        for h in range(2):
            chain_end(f + (n_fs - f) * (1 - jnp.minimum(1, f)), h)
        finish()
        sent(tokbuf.at[0], tok_s.at[0])
        sent(metabuf.at[0], meta_s.at[0])
        sent(wall.at[:, 0, pl.ds(0, half)], ws_s.at[0])

    @pl.when(inside)
    def _():
        for hop in (1, 2):
            meta_to(hop, f)
        for h in range(2):
            for hop in (1, 2):
                tokens_to(hop, f, h)
        start_up()
        for h in range(2):
            take_tokens(2, h, hop=1)
            take_tokens(1, h, hop=2)
        give_shared(1, (0,))
        give_shared(2)
        give_expert(2)
        forward_block(1)
        forward_block(2)
        hidden_block(0)
        for h in range(2):
            take_tokens(3, h, hop=1)
        give_shared(1, (1, 2))
        give_expert(1)
        forward_block(3)
        keep_own()
        for m in range(3):
            pass_shared(1, m, hop=2)
        give_expert(3)
        hidden_block(1)
        hidden_block(2)
        for m in range(3):
            pass_routed(1, m)
        down_block(0)
        hidden_block(3)
        pass_shared(2, 0, hop=1)
        pass_shared(2, 1, hop=1)
        down_block(1)
        down_block(2)
        down_block(3)
        pass_shared(2, 2, hop=1)
        for m in range(3):
            pass_routed(2, m)
        for m in range(3):
            pass_shared(3, m, hop=1)
        for m in range(3):
            pass_routed(3, m)
        for i in (3, 2, 1):
            for h in range(2):
                chain_on(i, h)
        for h in range(2):
            chain_end(f, h)
            chain_end(n_fs, h)
        finish()
        sent(chain, tok_s.at[0])
        sent(metabuf, meta_s.at[0])
        sent(wall.at[:, :, pl.ds(0, half)], ws_s.at[0])

    with scope("ywait"):
        landed(wout_ref.at[:, :, pl.ds(0, n_fs - 1), 0], yw_r.at[0])

    with scope("drain"):
        sent(ssbuf.at[three], ss_s.at[0])
        sent(scbuf.at[pl.ds(0, n_fs - 1)], sc_s.at[0])
        sent(rsbuf.at[:, three], rs_s.at[0])
        sent(hid.at[:, three], ag_s.at[0])
        sent(outb.at[pl.ds(0, n_fs - 1)], ch_s.at[0])
        sent(wout_ref.at[0, :, pl.ds(0, n_fs - 1), 0], we_s.at[0])
        sent(wout_ref.at[:, :, pl.ds(0, n_fs - 1), 0], yw_s.at[0])


def put_out(mixed_ref, served_ref, *rest):
    outs, sems = rest[:-1], rest[-1]
    copies = [pltpu.make_async_copy(served_ref.at[i], outs[1 + i], sems.at[1 + i]) for i in range(len(outs) - 1)]
    copies.append(pltpu.make_async_copy(mixed_ref, outs[0], sems.at[0]))
    for copy in copies:
        copy.start()
    for copy in copies:
        copy.wait()


def per_device_fused(
    tokens,
    routes,
    routing_weight,
    norm_gain_vector,
    expert_gate,
    expert_up,
    expert_down,
    shared_gate,
    shared_up,
    shared_down,
):
    n_fs, n_tp = lax.axis_size("fs"), lax.axis_size("tp")
    rows, width = tokens.shape
    experts, units, _ = expert_gate.shape
    top_count = routes.shape[1]
    sub, half = rows // n_tp, units // 2
    meta_rows = -(-2 * top_count // 8) * 8
    lanes = -(-rows // 128) * 128
    f32, bf16 = jnp.float32, jnp.bfloat16
    kinds = top_count + 1
    dma = pltpu.SemaphoreType.DMA
    vmem = pl.BlockSpec(memory_space=pltpu.VMEM)
    hbm = pl.BlockSpec(memory_space=pltpu.HBM)
    mixed, served = pl.pallas_call(
        functools.partial(fused_kernel, n_fs, n_tp, top_count),
        out_shape=(
            pltpu.VMEM((rows, width), bf16),
            pltpu.VMEM((2, 3, n_fs, 2, half, width), bf16),
        ),
        in_specs=[hbm] * 10,
        out_specs=(vmem, vmem),
        scratch_shapes=[
            pltpu.VMEM((3, experts + 1, units, width), f32),
            pltpu.VMEM((top_count, rows), jnp.int32),
            pltpu.VMEM((top_count, rows), f32),
            pltpu.VMEM((1, width), f32),
            pltpu.VMEM((3, experts + 1, units, width), bf16),
            pltpu.VMEM((n_fs, rows, width), bf16),
            pltpu.VMEM((meta_rows, lanes), f32),
            pltpu.VMEM((n_fs + 1, meta_rows, lanes), f32),
            pltpu.VMEM((8, lanes), f32),
            pltpu.VMEM((n_tp, 8, lanes), f32),
            pltpu.VMEM((8, lanes), f32),
            pltpu.VMEM((n_fs, 8, lanes), f32),
            pltpu.VMEM((n_fs, rows, meta_rows), f32),
            pltpu.VMEM((n_fs, rows, 8), f32),
            pltpu.VMEM((n_fs, n_tp, sub, 2 * kinds * units), bf16),
            pltpu.VMEM((n_fs, n_tp, sub, 2 * kinds * units), bf16),
            pltpu.VMEM((n_fs, n_tp, sub, kinds * units), bf16),
            pltpu.VMEM((n_fs, rows, width), f32),
            pltpu.VMEM((n_fs, rows, width), bf16),
            pltpu.VMEM((n_fs + 1, rows, width), bf16),
            dma((7,)),
            dma((1,)), dma((n_fs, 2)),
            dma((1,)), dma((n_fs,)),
            dma((1,)), dma((1,)),
            dma((1,)), dma((n_fs,)),
            dma((1,)), dma((n_fs,)),
            dma((1,)), dma((n_fs,)),
            dma((1,)), dma((n_fs + 1, 2)),
            dma((1,)), dma((n_fs, 3)),
            dma((1,)), dma((n_fs, 3)),
            dma((1,)), dma((1,)),
        ],
        compiler_params=pltpu.CompilerParams(
            collective_id=0, has_side_effects=True, vmem_limit_bytes=40 * 1024 * 1024
        ),
        name="hand_over_and_layer",
    )(*[
        pltpu.with_memory_space_constraint(value, pltpu.HBM)
        for value in (
            tokens, routes.T, routing_weight.T, norm_gain_vector[None, :],
            expert_gate, expert_up, expert_down, shared_gate, shared_up, shared_down,
        )
    ])
    units_all = n_fs * units
    outs = pl.pallas_call(
        put_out,
        out_shape=(
            jax.ShapeDtypeStruct((rows, width), bf16),
            *[jax.ShapeDtypeStruct((units_all, width), bf16)] * 6,
        ),
        in_specs=[vmem] * 2,
        out_specs=(hbm,) * 7,
        scratch_shapes=[dma((7,))],
        compiler_params=pltpu.CompilerParams(vmem_limit_bytes=8 * 1024 * 1024),
        name="put_out",
    )(mixed, served.reshape(6, units_all, width))
    return (outs[0], outs[1][None], outs[2][None], outs[3][None], *outs[4:])


def per_device(tokens, routes, routing_weight, norm_gain_vector, *weights):
    experts, units, width = weights[0].shape
    rows, n_fs, n_tp = tokens.shape[0], lax.axis_size("fs"), lax.axis_size("tp")
    whole_tiles = units % 128 == 0 and width % 128 == 0 and rows % (16 * n_tp) == 0
    fits = (experts + 1) * units * width <= 2**20 and n_fs == 4 and n_tp <= 4
    chosen = per_device_plain
    if whole_tiles and fits and experts == n_fs and lax.axis_size("grp") == 2:
        chosen = per_device_fused
    return chosen(tokens, routes, routing_weight, norm_gain_vector, *weights)


def solution(mesh):
    return jax.shard_map(
        per_device,
        mesh=mesh,
        in_specs=(
            P(("grp", "fs"), "tp"),
            P(("grp", "fs"), None),
            P(("grp", "fs"), None),
            P("tp"),
            P(None, "fs", "tp"),
            P(None, "fs", "tp"),
            P(None, "fs", "tp"),
            P("fs", "tp"),
            P("fs", "tp"),
            P("fs", "tp"),
        ),
        out_specs=(
            P(("grp", "fs"), "tp"),
            P(("grp", "fs"), None, "tp"),
            P(("grp", "fs"), None, "tp"),
            P(("grp", "fs"), None, "tp"),
            P("grp", "tp"),
            P("grp", "tp"),
            P("grp", "tp"),
        ),
        check_vma=False,
    )
```

time: 65.6 us -> 55.2 us (0.84)
  Pallas kernels: 64.8 us -> 54.4 us
    pallas_call x1, Pallas kernels: 63.1 us -> 52.6 us  [per_device_fused(): pl.pallas_call(functools.partial(fused_kernel, n_fs, n_tp, top_count), ou...]
where the time goes in v2:
time: 55.2 us; the launch traced here: 55 us
  Pallas kernels  54.4 us (99%)
  between operations  0.64 us (1%)
    pallas_call x1, Pallas kernels, per_device_fused(): pl.pallas_call(functools.partial(fused_kernel, n_fs, n_tp, top_count), ou...  52.6 us
    pallas_call x1, Pallas kernels, per_device_fused(): pl.pallas_call(put_out, out_shape=(jax.ShapeDtypeStruct((rows, width), bf...  1.78 us

profile of v2, /device:TPU:0, one launch (start us, length us, event | category | flops | bytes accessed | tf_op | source)
XLA Modules:
  0.0 55.0 jit_solution(8033528745320902588)
XLA Ops:
  0.6 52.6 %hand_over_and_layer.1 = (bf16[192,512]{1,0:T(8,128)(2,1)S(1)}, bf16[2,3,4,2,64,512]{5,4,3,2,1,0:T(8,128)(2,1)S(1)}) custom-call(bf16[192,512]{1,0:T(8,128)(2,1)} %tok_in.1, s32[2,192]{1,0:T(2,128)} %bitcast.8, f32[2,192]{1,0:T(2,128)} %bitcast.9, f32[1,512]{1,0:T(1,128)} %bitcast.10, f32[4,128,512]{2,1,0:T(8,128)} %eg_in.1, f32[4,128,512]{2,1,0:T(8,128)} %eu_in.1, ...), custom_call_target="tpu_custom_call" | custom-call | tf_op jit(solution)/shard_map/hand_over_and_layer/pallas_call | solution.py:535
  53.3 1.8 %put_out.1 = (bf16[192,512]{1,0:T(8,128)(2,1)}, bf16[512,512]{1,0:T(8,128)(2,1)}, bf16[512,512]{1,0:T(8,128)(2,1)}, bf16[512,512]{1,0:T(8,128)(2,1)}, bf16[512,5...) custom-call(bf16[192,512]{1,0:T(8,128)(2,1)S(1)} %get-tuple-element.16.mixed_ref, ...), custom_call_target="tpu_custom_call" | custom-call | tf_op jit(solution)/shard_map/put_out/pallas_call | solution.py:588

commit v3 on v2

--- a/solution.py
+++ b/solution.py
@@ -126,8 +126,8 @@
     tok_in, routes_in, weight_in, gain_in, eg_in, eu_in, ed_in, sg_in, su_in, sd_in,
     mixed_ref, wout_ref,
     raw, routes_ref, weight_ref, gain_ref,
-    wall, tokbuf, meta_ref, metabuf, ssown, ssbuf, scown, scbuf, mt, sct, part, rsbuf, hid, acc, outb, chain,
-    in_s, tok_s, tok_r, meta_s, meta_r, ss_s, ss_r, sc_s, sc_r, rs_s, rs_r, ag_s, ag_r,
+    wall, tokbuf, meta_ref, metabuf, ssown, ssbuf, mt, part, rsbuf, hid, acc, outb, chain,
+    in_s, tok_s, tok_r, meta_s, meta_r, ss_s, ss_r, rs_s, rs_r, ag_s, ag_r,
     ch_s, ch_r, we_s, we_r, ws_s, ws_r, yw_s, yw_r,
 ):
     g, f, t = lax.axis_index("grp"), lax.axis_index("fs"), lax.axis_index("tp")
@@ -173,13 +173,23 @@
     def landed(ref, recv):
         remote(ref, ref, recv, recv, partner).wait_recv()
 
-    fs_others = [lax.rem(f + j, n_fs) for j in range(1, n_fs)]
     tp_others = [lax.rem(t + j, n_tp) for j in range(1, n_tp)]
 
     barrier = pltpu.get_barrier_semaphore()
-    peers = [at_fs(d) for d in fs_others] + [at_tp(d) for d in tp_others] + [partner]
-    for device in peers:
+
+    def greet(device):
         pl.semaphore_signal(barrier, inc=1, device_id=device, device_id_type=MESH)
+
+    @pl.when(f > 0)
+    def _():
+        greet(at_fs(f - 1))
+
+    @pl.when(f < n_fs - 1)
+    def _():
+        greet(at_fs(f + 1))
+
+    for device in [at_tp(d) for d in tp_others] + [partner]:
+        greet(device)
 
     small = [
         pltpu.make_async_copy(tok_in, tokbuf.at[f], in_s.at[0]),
@@ -192,22 +202,9 @@
     for m, (routed, shared) in enumerate(((eg_in, sg_in), (eu_in, su_in), (ed_in, sd_in))):
         pltpu.make_async_copy(routed, raw.at[m, pl.ds(0, experts)], in_s.at[4 + m]).start()
         pltpu.make_async_copy(shared, raw.at[m, experts], in_s.at[4 + m]).start()
-    for load in small:
-        load.wait()
-    meta_ref[...] = jnp.zeros(meta_ref.shape, f32)
-    meta_ref[0:top_count, 0:rows] = routes_ref[...].astype(f32)
-    meta_ref[top_count : 2 * top_count, 0:rows] = weight_ref[...]
-
-    x = tokbuf[f].astype(f32)
-    sq = x * x
-    high = sq.astype(bf16)
-    low = (sq - high.astype(f32)).astype(bf16)
-    ones = jnp.ones((8, width), bf16)
-    ssown[...] = jnp.zeros(ssown.shape, f32)
-    ssown[:, 0:rows] = dense_rows(ones, high) + dense_rows(ones, low)
-
+    small[0].wait()
     with scope("barrier"):
-        pl.semaphore_wait(barrier, len(peers))
+        pl.semaphore_wait(barrier, n_tp + jnp.minimum(1, f) + jnp.minimum(1, n_fs - 1 - f))
 
     def convert(m):
         pltpu.make_async_copy(raw.at[m], raw.at[m], in_s.at[4 + m]).wait()
@@ -240,14 +237,10 @@
                 remote(part.at[i, d], rsbuf.at[i, t], rs_s.at[0], rs_r.at[i], at_tp(d)).start()
 
     def hidden_block(i):
-        s = source(i)
         with scope(f"hid{i}"):
-            if i > 0:
-                landed(scbuf.at[s], sc_r.at[s])
-            sct[i] = transposed(scown if i == 0 else scbuf.at[s])
             own_rows = pl.ds(pl.multiple_of(t * sub, 8), sub)
-            scale = sct[i, own_rows, 0:1]
             weights = mt[i, own_rows, :]
+            scale = weights[:, 2 * top_count : 2 * top_count + 1]
             landed(rsbuf.at[i, three], rs_r.at[i])
             total = part[i, t].astype(f32)
             for d in tp_others:
@@ -317,13 +310,16 @@
     def take_tokens(i, h, hop=None):
         s = source(i)
         with scope(f"tok{i}{h}"):
-            if h == 0:
-                landed(metabuf.at[s], meta_r.at[s])
-                if hop:
-                    meta_to(hop, s)
             landed(tokbuf.at[s, parts[h]], tok_r.at[s, h])
             if hop:
                 tokens_to(hop, s, h)
+
+    def take_small(i, hop=None):
+        s = source(i)
+        with scope(f"small{i}"):
+            landed(metabuf.at[s], meta_r.at[s])
+            if hop:
+                meta_to(hop, s)
 
     mine = pl.ds(pl.multiple_of(g * half, 16), half)
 
@@ -354,7 +350,19 @@
             landed(ref, we_r.at[s, m])
         remote(ref, ref, yw_s.at[0], yw_r.at[0], partner).start()
 
-    def start_up():
+    def start_up(hops):
+        for load in small[1:]:
+            load.wait()
+        meta_ref[...] = jnp.zeros(meta_ref.shape, f32)
+        meta_ref[0:top_count, 0:rows] = routes_ref[...].astype(f32)
+        meta_ref[top_count : 2 * top_count, 0:rows] = weight_ref[...]
+        x = tokbuf[f].astype(f32)
+        sq = x * x
+        high = sq.astype(bf16)
+        low = (sq - high.astype(f32)).astype(bf16)
+        ones = jnp.ones((8, width), bf16)
+        ssown[...] = jnp.zeros(ssown.shape, f32)
+        ssown[:, 0:rows] = dense_rows(ones, high) + dense_rows(ones, low)
         for d in tp_others:
             remote(ssown, ssbuf.at[t], ss_s.at[0], ss_r.at[0], at_tp(d)).start()
         convert(0)
@@ -365,9 +373,11 @@
             landed(ssbuf.at[three], ss_r.at[0])
         for d in tp_others:
             squares = squares + ssbuf[d]
-        scown[...] = lax.rsqrt(squares / (width * n_tp) + norm_eps)
-        for d in fs_others:
-            remote(scown, scbuf.at[f], sc_s.at[0], sc_r.at[f], at_fs(d)).start()
+        scale = lax.rsqrt(squares / (width * n_tp) + norm_eps)
+        meta_ref[2 * top_count : 2 * top_count + 1] = scale[0:1]
+        for hop in hops:
+            meta_to(hop, f)
+        mt[0] = transposed(meta_ref)
         convert(2)
 
     def keep_own():
@@ -380,47 +390,52 @@
 
     @pl.when(at_edge)
     def _():
-        meta_to(1, f)
         for h in range(2):
             tokens_to(1, f, h)
-        start_up()
+        start_up((1,))
         give_shared(1)
-        for i in range(1, n_fs):
-            give_expert(i)
+        give_expert(1)
         keep_own()
         take_tokens(1, 0)
         take_tokens(1, 1)
+        take_small(1)
+        give_expert(2)
         forward_block(1)
         hidden_block(0)
         take_tokens(2, 0)
         take_tokens(2, 1)
+        take_small(2)
+        give_expert(3)
         forward_block(2)
         hidden_block(1)
         down_block(0)
         pass_shared(1, 0)
         take_tokens(3, 0)
         take_tokens(3, 1)
+        take_small(3)
         forward_block(3)
         hidden_block(2)
         down_block(1)
         chain_start(1)
         pass_shared(1, 1)
+        pass_shared(1, 2)
         pass_routed(3, 0)
         hidden_block(3)
         pass_routed(3, 1)
         pass_routed(3, 2)
         down_block(2)
-        pass_shared(1, 2)
+        pass_routed(1, 0)
         down_block(3)
         chain_start(3)
         chain_start(2)
-        for m in range(3):
-            pass_routed(1, m)
+        pass_routed(1, 1)
+        pass_routed(1, 2)
         pass_shared(2, 0)
         pass_shared(2, 1)
-        for m in range(3):
-            pass_routed(2, m)
+        pass_routed(2, 0)
         pass_shared(2, 2)
+        pass_routed(2, 1)
+        pass_routed(2, 2)
         for m in range(3):
             pass_shared(3, m)
         for h in range(2):
@@ -432,15 +447,15 @@
 
     @pl.when(inside)
     def _():
-        for hop in (1, 2):
-            meta_to(hop, f)
         for h in range(2):
             for hop in (1, 2):
                 tokens_to(hop, f, h)
-        start_up()
+        start_up((1, 2))
         for h in range(2):
             take_tokens(2, h, hop=1)
             take_tokens(1, h, hop=2)
+        take_small(2, hop=1)
+        take_small(1, hop=2)
         give_shared(1, (0,))
         give_shared(2)
         give_expert(2)
@@ -449,6 +464,7 @@
         hidden_block(0)
         for h in range(2):
             take_tokens(3, h, hop=1)
+        take_small(3, hop=1)
         give_shared(1, (1, 2))
         give_expert(1)
         forward_block(3)
@@ -474,9 +490,8 @@
             pass_shared(3, m, hop=1)
         for m in range(3):
             pass_routed(3, m)
-        for i in (3, 2, 1):
-            for h in range(2):
-                chain_on(i, h)
+        for i, h in ((3, 0), (3, 1), (2, 0), (1, 0), (2, 1), (1, 1)):
+            chain_on(i, h)
         for h in range(2):
             chain_end(f, h)
             chain_end(n_fs, h)
@@ -490,7 +505,6 @@
 
     with scope("drain"):
         sent(ssbuf.at[three], ss_s.at[0])
-        sent(scbuf.at[pl.ds(0, n_fs - 1)], sc_s.at[0])
         sent(rsbuf.at[:, three], rs_s.at[0])
         sent(hid.at[:, three], ag_s.at[0])
         sent(outb.at[pl.ds(0, n_fs - 1)], ch_s.at[0])
@@ -525,7 +539,7 @@
     experts, units, _ = expert_gate.shape
     top_count = routes.shape[1]
     sub, half = rows // n_tp, units // 2
-    meta_rows = -(-2 * top_count // 8) * 8
+    meta_rows = -(-(2 * top_count + 1) // 8) * 8
     lanes = -(-rows // 128) * 128
     f32, bf16 = jnp.float32, jnp.bfloat16
     kinds = top_count + 1
@@ -551,10 +565,7 @@
             pltpu.VMEM((n_fs + 1, meta_rows, lanes), f32),
             pltpu.VMEM((8, lanes), f32),
             pltpu.VMEM((n_tp, 8, lanes), f32),
-            pltpu.VMEM((8, lanes), f32),
-            pltpu.VMEM((n_fs, 8, lanes), f32),
             pltpu.VMEM((n_fs, rows, meta_rows), f32),
-            pltpu.VMEM((n_fs, rows, 8), f32),
             pltpu.VMEM((n_fs, n_tp, sub, 2 * kinds * units), bf16),
             pltpu.VMEM((n_fs, n_tp, sub, 2 * kinds * units), bf16),
             pltpu.VMEM((n_fs, n_tp, sub, kinds * units), bf16),
@@ -565,7 +576,6 @@
             dma((1,)), dma((n_fs, 2)),
             dma((1,)), dma((n_fs,)),
             dma((1,)), dma((1,)),
-            dma((1,)), dma((n_fs,)),
             dma((1,)), dma((n_fs,)),
             dma((1,)), dma((n_fs,)),
             dma((1,)), dma((n_fs + 1, 2)),

time: 55.2 us -> 53.9 us (0.976)
  Pallas kernels: 54.4 us -> 53.1 us
    pallas_call x1, Pallas kernels: 52.6 us -> 51.3 us  [per_device_fused(): pl.pallas_call(functools.partial(fused_kernel, n_fs, n_tp, top_count), ou...]
where the time goes in v3:
time: 53.9 us; the launch traced here: 53.7 us
  Pallas kernels  53.1 us (99%)
  between operations  0.64 us (1%)
    pallas_call x1, Pallas kernels, per_device_fused(): pl.pallas_call(functools.partial(fused_kernel, n_fs, n_tp, top_count), ou...  51.3 us
    pallas_call x1, Pallas kernels, per_device_fused(): pl.pallas_call(put_out, out_shape=(jax.ShapeDtypeStruct((rows, width), bf...  1.78 us

profile of v3, /device:TPU:0, one launch (start us, length us, event | category | flops | bytes accessed | tf_op | source)
XLA Modules:
  0.0 53.7 jit_solution(5941108569857871709)
XLA Ops:
  0.6 51.3 %hand_over_and_layer.1 = (bf16[192,512]{1,0:T(8,128)(2,1)S(1)}, bf16[2,3,4,2,64,512]{5,4,3,2,1,0:T(8,128)(2,1)S(1)}) custom-call(bf16[192,512]{1,0:T(8,128)(2,1)} %tok_in.1, s32[2,192]{1,0:T(2,128)} %bitcast.8, f32[2,192]{1,0:T(2,128)} %bitcast.9, f32[1,512]{1,0:T(1,128)} %bitcast.10, f32[4,128,512]{2,1,0:T(8,128)} %eg_in.1, f32[4,128,512]{2,1,0:T(8,128)} %eu_in.1, ...), custom_call_target="tpu_custom_call" | custom-call | tf_op jit(solution)/shard_map/hand_over_and_layer/pallas_call | solution.py:549
  52.0 1.8 %put_out.1 = (bf16[192,512]{1,0:T(8,128)(2,1)}, bf16[512,512]{1,0:T(8,128)(2,1)}, bf16[512,512]{1,0:T(8,128)(2,1)}, bf16[512,512]{1,0:T(8,128)(2,1)}, bf16[512,5...) custom-call(bf16[192,512]{1,0:T(8,128)(2,1)S(1)} %get-tuple-element.16.mixed_ref, ...), custom_call_target="tpu_custom_call" | custom-call | tf_op jit(solution)/shard_map/put_out/pallas_call | solution.py:598

commit v4 on v3

--- a/solution.py
+++ b/solution.py
@@ -126,19 +126,20 @@
     tok_in, routes_in, weight_in, gain_in, eg_in, eu_in, ed_in, sg_in, su_in, sd_in,
     mixed_ref, wout_ref,
     raw, routes_ref, weight_ref, gain_ref,
-    wall, tokbuf, meta_ref, metabuf, ssown, ssbuf, mt, part, rsbuf, hid, acc, outb, chain,
+    wall, tokbuf, meta_ref, metabuf, ssown, ssbuf, mt, part, rsbuf, hid, part_a, rsbuf_a, hid_a, part_b, rsbuf_b, hid_b, acc, outb, chain,
     in_s, tok_s, tok_r, meta_s, meta_r, ss_s, ss_r, rs_s, rs_r, ag_s, ag_r,
     ch_s, ch_r, we_s, we_r, ws_s, ws_r, yw_s, yw_r,
 ):
     g, f, t = lax.axis_index("grp"), lax.axis_index("fs"), lax.axis_index("tp")
     rows, width = tokbuf.shape[1:]
     experts, units = eg_in.shape[0], eg_in.shape[1]
-    sub = rows // n_tp
+    pieces = 3
+    row_step = rows // pieces
     half = units // 2
     f32, bf16 = jnp.float32, jnp.bfloat16
     code = outward_first(n_fs)
     scope = jax.named_scope
-    parts = [pl.ds(h * (rows // 2), rows // 2) for h in range(2)]
+    parts = [pl.ds(h * row_step, row_step) for h in range(pieces)]
     three = pl.ds(0, n_tp - 1)
 
     def source(i):
@@ -215,36 +216,47 @@
     def transposed(row_ref):
         return jnp.transpose(row_ref[...])[0:rows]
 
-    def forward_block(i):
+    segments = [
+        (i, 0, rows, part.at[i], rsbuf.at[i], hid.at[i]) for i in range(n_fs - 1)
+    ] + [
+        (n_fs - 1, 0, 2 * row_step, part_a, rsbuf_a, hid_a),
+        (n_fs - 1, 2 * row_step, row_step, part_b, rsbuf_b, hid_b),
+    ]
+
+    def forward_block(q):
+        i, first, count, part, rsbuf, _ = segments[q]
+        span = pl.ds(first, count)
         s = source(i)
-        with scope(f"fwd{i}"):
-            mt[i] = transposed(meta_ref if i == 0 else metabuf.at[s])
-            tokens = tokbuf[s]
-            names = [mt[i, :, k : k + 1] for k in range(top_count)]
+        with scope(f"fwd{q}"):
+            if first == 0:
+                mt[i] = transposed(meta_ref if i == 0 else metabuf.at[s])
+            tokens = tokbuf[s, span]
+            names = [mt[i, span, k : k + 1] for k in range(top_count)]
             columns = []
             for m in range(2):
                 weight = wall[m].reshape((experts + 1) * units, width)
                 sums = dense_rows(tokens, weight)
                 for name in names:
-                    chosen = jnp.zeros((rows, units), f32)
+                    chosen = jnp.zeros((count, units), f32)
                     for e in range(experts):
                         chosen = jnp.where(name == float(e), sums[:, e * units : (e + 1) * units], chosen)
                     columns.append(chosen)
                 columns.append(sums[:, experts * units :])
             for c, column in enumerate(columns):
-                part[i, :, :, c * units : (c + 1) * units] = column.astype(bf16).reshape(n_tp, sub, units)
+                part[:, :, c * units : (c + 1) * units] = column.astype(bf16).reshape(n_tp, count // n_tp, units)
             for d in tp_others:
-                remote(part.at[i, d], rsbuf.at[i, t], rs_s.at[0], rs_r.at[i], at_tp(d)).start()
-
-    def hidden_block(i):
-        with scope(f"hid{i}"):
-            own_rows = pl.ds(pl.multiple_of(t * sub, 8), sub)
-            weights = mt[i, own_rows, :]
+                remote(part.at[d], rsbuf.at[t], rs_s.at[0], rs_r.at[q], at_tp(d)).start()
+
+    def hidden_block(q):
+        i, first, count, part, rsbuf, hid = segments[q]
+        sub = count // n_tp
+        with scope(f"hid{q}"):
+            weights = mt[i, pl.ds(pl.multiple_of(first + t * sub, 8), sub), :]
             scale = weights[:, 2 * top_count : 2 * top_count + 1]
-            landed(rsbuf.at[i, three], rs_r.at[i])
-            total = part[i, t].astype(f32)
+            landed(rsbuf.at[three], rs_r.at[q])
+            total = part[t].astype(f32)
             for d in tp_others:
-                total = total + rsbuf[i, d].astype(f32)
+                total = total + rsbuf[d].astype(f32)
             total = total * scale
             kinds = top_count + 1
             for k in range(kinds):
@@ -253,24 +265,26 @@
                 value = jax.nn.silu(gate) * up
                 if k < top_count:
                     value = value * weights[:, top_count + k : top_count + k + 1]
-                hid[i, t, :, k * units : (k + 1) * units] = value.astype(bf16)
+                hid[t, :, k * units : (k + 1) * units] = value.astype(bf16)
             for d in tp_others:
-                remote(hid.at[i, t], hid.at[i, t], ag_s.at[0], ag_r.at[i], at_tp(d)).start()
-
-    def down_block(i):
-        with scope(f"down{i}"):
-            landed(hid.at[i, three], ag_r.at[i])
-            values = hid[i].astype(f32).reshape(rows, (top_count + 1) * units)
-            names = [mt[i, :, k : k + 1] for k in range(top_count)]
+                remote(hid.at[t], hid.at[t], ag_s.at[0], ag_r.at[q], at_tp(d)).start()
+
+    def down_block(q):
+        i, first, count, _, _, hid = segments[q]
+        span = pl.ds(first, count)
+        with scope(f"down{q}"):
+            landed(hid.at[three], ag_r.at[q])
+            values = hid[...].astype(f32).reshape(count, (top_count + 1) * units)
+            names = [mt[i, span, k : k + 1] for k in range(top_count)]
             spread = []
             for e in range(experts):
-                chosen = jnp.zeros((rows, units), f32)
+                chosen = jnp.zeros((count, units), f32)
                 for k, name in enumerate(names):
                     chosen = jnp.where(name == float(e), values[:, k * units : (k + 1) * units], chosen)
                 spread.append(chosen.astype(bf16))
             spread.append(values[:, top_count * units :].astype(bf16))
             weight = wall[2].reshape((experts + 1) * units, width)
-            acc[i] = jnp.dot(jnp.concatenate(spread, axis=1), weight, preferred_element_type=f32)
+            acc[i, span] = jnp.dot(jnp.concatenate(spread, axis=1), weight, preferred_element_type=f32)
 
     def chain_send(i, h, hop, last):
         d = source(i)
@@ -281,8 +295,8 @@
             outb.at[i, parts[h]], chain.at[slot, parts[h]], ch_s.at[0], ch_r.at[slot, h], at_fs(source(hop))
         ).start()
 
-    def chain_start(i):
-        for h in range(2):
+    def chain_start(i, which=(0, 1, 2)):
+        for h in which:
             outb[i, parts[h]] = acc[i, parts[h]].astype(bf16)
             chain_send(i, h, 1, i == 1)
 
@@ -329,9 +343,9 @@
                 wall.at[m, experts, mine], wout_ref.at[1, m, f, g], ws_s.at[0], ws_r.at[f, m], at_fs(source(hop))
             ).start()
 
-    def give_expert(i):
+    def give_expert(i, pieces=(0, 1, 2)):
         d = source(i)
-        for m in range(3):
+        for m in pieces:
             remote(wall.at[m, d, mine], wout_ref.at[0, m, f, g], we_s.at[0], we_r.at[f, m], at_fs(d)).start()
 
     def pass_shared(i, m, hop=None):
@@ -366,7 +380,13 @@
         for d in tp_others:
             remote(ssown, ssbuf.at[t], ss_s.at[0], ss_r.at[0], at_tp(d)).start()
         convert(0)
+        if len(hops) > 1:
+            give_shared(1, (0,))
+            give_shared(2, (0,))
         convert(1)
+        if len(hops) > 1:
+            give_shared(1, (1,))
+            tokens_to(1, f, 0)
         forward_block(0)
         squares = ssown[...]
         with scope("sswait"):
@@ -390,55 +410,70 @@
 
     @pl.when(at_edge)
     def _():
-        for h in range(2):
+        for h in range(pieces):
             tokens_to(1, f, h)
         start_up((1,))
         give_shared(1)
         give_expert(1)
         keep_own()
-        take_tokens(1, 0)
-        take_tokens(1, 1)
+        pass_shared(1, 0)
+        pass_shared(1, 1)
+        take_tokens(2, 0)
+        give_expert(2)
+        hidden_block(0)
+        take_tokens(2, 1)
+        take_tokens(2, 2)
+        take_small(2)
+        forward_block(2)
+        down_block(0)
+        pass_shared(1, 2)
+        pass_routed(1, 0)
+        take_tokens(3, 0)
+
+        @pl.when(f > 0)
+        def _():
+            give_expert(3)
+
+        pass_routed(1, 1)
+        take_tokens(3, 1)
+        take_tokens(3, 2)
+        take_small(3)
+
+        @pl.when(f == 0)
+        def _():
+            give_expert(3)
+
+        forward_block(3)
+        forward_block(4)
+        hidden_block(2)
+        pass_routed(3, 0)
+        pass_routed(3, 1)
+        hidden_block(3)
+        hidden_block(4)
+        pass_routed(3, 2)
         take_small(1)
-        give_expert(2)
+        for h in range(pieces):
+            take_tokens(1, h)
         forward_block(1)
-        hidden_block(0)
-        take_tokens(2, 0)
-        take_tokens(2, 1)
-        take_small(2)
-        give_expert(3)
-        forward_block(2)
+        pass_routed(1, 2)
+        down_block(3)
+        chain_start(3, (0, 1))
+        pass_shared(2, 0)
+        down_block(4)
+        chain_start(3, (2,))
+        down_block(2)
+        chain_start(2)
+        pass_shared(2, 1)
         hidden_block(1)
-        down_block(0)
-        pass_shared(1, 0)
-        take_tokens(3, 0)
-        take_tokens(3, 1)
-        take_small(3)
-        forward_block(3)
-        hidden_block(2)
+        pass_routed(2, 0)
+        pass_routed(2, 1)
+        pass_shared(2, 2)
+        pass_routed(2, 2)
         down_block(1)
         chain_start(1)
-        pass_shared(1, 1)
-        pass_shared(1, 2)
-        pass_routed(3, 0)
-        hidden_block(3)
-        pass_routed(3, 1)
-        pass_routed(3, 2)
-        down_block(2)
-        pass_routed(1, 0)
-        down_block(3)
-        chain_start(3)
-        chain_start(2)
-        pass_routed(1, 1)
-        pass_routed(1, 2)
-        pass_shared(2, 0)
-        pass_shared(2, 1)
-        pass_routed(2, 0)
-        pass_shared(2, 2)
-        pass_routed(2, 1)
-        pass_routed(2, 2)
         for m in range(3):
             pass_shared(3, m)
-        for h in range(2):
+        for h in range(pieces):
             chain_end(f + (n_fs - f) * (1 - jnp.minimum(1, f)), h)
         finish()
         sent(tokbuf.at[0], tok_s.at[0])
@@ -447,27 +482,30 @@
 
     @pl.when(inside)
     def _():
-        for h in range(2):
-            for hop in (1, 2):
-                tokens_to(hop, f, h)
+        for h in range(pieces):
+            tokens_to(2, f, h)
         start_up((1, 2))
-        for h in range(2):
+        for h in range(pieces):
             take_tokens(2, h, hop=1)
             take_tokens(1, h, hop=2)
         take_small(2, hop=1)
         take_small(1, hop=2)
-        give_shared(1, (0,))
-        give_shared(2)
+        give_shared(1, (2,))
+        give_expert(1, (0, 1))
+        give_shared(2, (1, 2))
         give_expert(2)
         forward_block(1)
         forward_block(2)
         hidden_block(0)
-        for h in range(2):
-            take_tokens(3, h, hop=1)
+        take_tokens(3, 0, hop=1)
+        take_tokens(3, 1, hop=1)
+        take_tokens(3, 2, hop=1)
         take_small(3, hop=1)
-        give_shared(1, (1, 2))
-        give_expert(1)
+        for h in range(1, pieces):
+            tokens_to(1, f, h)
+        give_expert(1, (2,))
         forward_block(3)
+        forward_block(4)
         keep_own()
         for m in range(3):
             pass_shared(1, m, hop=2)
@@ -478,11 +516,13 @@
             pass_routed(1, m)
         down_block(0)
         hidden_block(3)
+        hidden_block(4)
         pass_shared(2, 0, hop=1)
         pass_shared(2, 1, hop=1)
         down_block(1)
         down_block(2)
         down_block(3)
+        down_block(4)
         pass_shared(2, 2, hop=1)
         for m in range(3):
             pass_routed(2, m)
@@ -490,9 +530,9 @@
             pass_shared(3, m, hop=1)
         for m in range(3):
             pass_routed(3, m)
-        for i, h in ((3, 0), (3, 1), (2, 0), (1, 0), (2, 1), (1, 1)):
+        for i, h in ((3, 0), (3, 1), (3, 2), (2, 0), (1, 0), (2, 1), (1, 1), (2, 2), (1, 2)):
             chain_on(i, h)
-        for h in range(2):
+        for h in range(pieces):
             chain_end(f, h)
             chain_end(n_fs, h)
         finish()
@@ -505,8 +545,8 @@
 
     with scope("drain"):
         sent(ssbuf.at[three], ss_s.at[0])
-        sent(rsbuf.at[:, three], rs_s.at[0])
-        sent(hid.at[:, three], ag_s.at[0])
+        sent(part, rs_s.at[0])
+        sent(hid, ag_s.at[0])
         sent(outb.at[pl.ds(0, n_fs - 1)], ch_s.at[0])
         sent(wout_ref.at[0, :, pl.ds(0, n_fs - 1), 0], we_s.at[0])
         sent(wout_ref.at[:, :, pl.ds(0, n_fs - 1), 0], yw_s.at[0])
@@ -538,7 +578,7 @@
     rows, width = tokens.shape
     experts, units, _ = expert_gate.shape
     top_count = routes.shape[1]
-    sub, half = rows // n_tp, units // 2
+    half = units // 2
     meta_rows = -(-(2 * top_count + 1) // 8) * 8
     lanes = -(-rows // 128) * 128
     f32, bf16 = jnp.float32, jnp.bfloat16
@@ -566,19 +606,21 @@
             pltpu.VMEM((8, lanes), f32),
             pltpu.VMEM((n_tp, 8, lanes), f32),
             pltpu.VMEM((n_fs, rows, meta_rows), f32),
-            pltpu.VMEM((n_fs, n_tp, sub, 2 * kinds * units), bf16),
-            pltpu.VMEM((n_fs, n_tp, sub, 2 * kinds * units), bf16),
-            pltpu.VMEM((n_fs, n_tp, sub, kinds * units), bf16),
+            *[
+                pltpu.VMEM(lead + (n_tp, count // n_tp, times * kinds * units), bf16)
+                for lead, count in (((n_fs - 1,), rows), ((), 2 * rows // 3), ((), rows // 3))
+                for times in (2, 2, 1)
+            ],
             pltpu.VMEM((n_fs, rows, width), f32),
             pltpu.VMEM((n_fs, rows, width), bf16),
             pltpu.VMEM((n_fs + 1, rows, width), bf16),
             dma((7,)),
-            dma((1,)), dma((n_fs, 2)),
+            dma((1,)), dma((n_fs, 3)),
             dma((1,)), dma((n_fs,)),
             dma((1,)), dma((1,)),
-            dma((1,)), dma((n_fs,)),
-            dma((1,)), dma((n_fs,)),
-            dma((1,)), dma((n_fs + 1, 2)),
+            dma((1,)), dma((n_fs + 1,)),
+            dma((1,)), dma((n_fs + 1,)),
+            dma((1,)), dma((n_fs + 1, 3)),
             dma((1,)), dma((n_fs, 3)),
             dma((1,)), dma((n_fs, 3)),
             dma((1,)), dma((1,)),
@@ -613,7 +655,7 @@
 def per_device(tokens, routes, routing_weight, norm_gain_vector, *weights):
     experts, units, width = weights[0].shape
     rows, n_fs, n_tp = tokens.shape[0], lax.axis_size("fs"), lax.axis_size("tp")
-    whole_tiles = units % 128 == 0 and width % 128 == 0 and rows % (16 * n_tp) == 0
+    whole_tiles = units % 128 == 0 and width % 128 == 0 and rows % (48 * n_tp) == 0
     fits = (experts + 1) * units * width <= 2**20 and n_fs == 4 and n_tp <= 4
     chosen = per_device_plain
     if whole_tiles and fits and experts == n_fs and lax.axis_size("grp") == 2:

time: 53.9 us -> 53.6 us (level)
  no operation moved by 1% of the time
where the time goes in v4:
time: 53.6 us; the launch traced here: 53.4 us
  Pallas kernels  52.8 us (99%)
  between operations  0.64 us (1%)
    pallas_call x1, Pallas kernels, per_device_fused(): pl.pallas_call(functools.partial(fused_kernel, n_fs, n_tp, top_count), ou...  51 us
    pallas_call x1, Pallas kernels, per_device_fused(): pl.pallas_call(put_out, out_shape=(jax.ShapeDtypeStruct((rows, width), bf...  1.78 us

profile of v4, /device:TPU:0, one launch (start us, length us, event | category | flops | bytes accessed | tf_op | source)
XLA Modules:
  0.0 53.4 jit_solution(8749221696354338282)
XLA Ops:
  0.6 51.0 %hand_over_and_layer.1 = (bf16[192,512]{1,0:T(8,128)(2,1)S(1)}, bf16[2,3,4,2,64,512]{5,4,3,2,1,0:T(8,128)(2,1)S(1)}) custom-call(bf16[192,512]{1,0:T(8,128)(2,1)} %tok_in.1, s32[2,192]{1,0:T(2,128)} %bitcast.8, f32[2,192]{1,0:T(2,128)} %bitcast.9, f32[1,512]{1,0:T(1,128)} %bitcast.10, f32[4,128,512]{2,1,0:T(8,128)} %eg_in.1, f32[4,128,512]{2,1,0:T(8,128)} %eu_in.1, ...), custom_call_target="tpu_custom_call" | custom-call | tf_op jit(solution)/shard_map/hand_over_and_layer/pallas_call | solution.py:589
  51.7 1.8 %put_out.1 = (bf16[192,512]{1,0:T(8,128)(2,1)}, bf16[512,512]{1,0:T(8,128)(2,1)}, bf16[512,512]{1,0:T(8,128)(2,1)}, bf16[512,512]{1,0:T(8,128)(2,1)}, bf16[512,5...) custom-call(bf16[192,512]{1,0:T(8,128)(2,1)S(1)} %get-tuple-element.16.mixed_ref, ...), custom_call_target="tpu_custom_call" | custom-call | tf_op jit(solution)/shard_map/put_out/pallas_call | solution.py:640

commit v5 on v4

--- a/solution.py
+++ b/solution.py
@@ -554,12 +554,15 @@
 
 def put_out(mixed_ref, served_ref, *rest):
     outs, sems = rest[:-1], rest[-1]
-    copies = [pltpu.make_async_copy(served_ref.at[i], outs[1 + i], sems.at[1 + i]) for i in range(len(outs) - 1)]
-    copies.append(pltpu.make_async_copy(mixed_ref, outs[0], sems.at[0]))
-    for copy in copies:
-        copy.start()
-    for copy in copies:
-        copy.wait()
+    step = served_ref.shape[1] // 4
+    for i in range(len(outs) - 1):
+        for j in range(4):
+            span = pl.ds(j * step, step)
+            pltpu.make_async_copy(served_ref.at[i, span], outs[1 + i].at[span], sems.at[1 + i]).start()
+    pltpu.make_async_copy(mixed_ref, outs[0], sems.at[0]).start()
+    for i in range(len(outs) - 1):
+        pltpu.make_async_copy(served_ref.at[i], outs[1 + i], sems.at[1 + i]).wait()
+    pltpu.make_async_copy(mixed_ref, outs[0], sems.at[0]).wait()
 
 
 def per_device_fused(

time: 53.6 us -> 53.6 us (level)
  no operation moved by 1% of the time
where the time goes in v5:
time: 53.6 us; the launch traced here: 53.4 us
  Pallas kernels  52.8 us (99%)
  between operations  0.64 us (1%)
    pallas_call x1, Pallas kernels, per_device_fused(): pl.pallas_call(functools.partial(fused_kernel, n_fs, n_tp, top_count), ou...  51 us
    pallas_call x1, Pallas kernels, per_device_fused(): pl.pallas_call(put_out, out_shape=(jax.ShapeDtypeStruct((rows, width), bf...  1.77 us

profile of v5, /device:TPU:0, one launch (start us, length us, event | category | flops | bytes accessed | tf_op | source)
XLA Modules:
  0.0 53.4 jit_solution(8672517110674173479)
XLA Ops:
  0.6 51.0 %hand_over_and_layer.1 = (bf16[192,512]{1,0:T(8,128)(2,1)S(1)}, bf16[2,3,4,2,64,512]{5,4,3,2,1,0:T(8,128)(2,1)S(1)}) custom-call(bf16[192,512]{1,0:T(8,128)(2,1)} %tok_in.1, s32[2,192]{1,0:T(2,128)} %bitcast.8, f32[2,192]{1,0:T(2,128)} %bitcast.9, f32[1,512]{1,0:T(1,128)} %bitcast.10, f32[4,128,512]{2,1,0:T(8,128)} %eg_in.1, f32[4,128,512]{2,1,0:T(8,128)} %eu_in.1, ...), custom_call_target="tpu_custom_call" | custom-call | tf_op jit(solution)/shard_map/hand_over_and_layer/pallas_call | solution.py:592
  51.7 1.8 %put_out.1 = (bf16[192,512]{1,0:T(8,128)(2,1)}, bf16[512,512]{1,0:T(8,128)(2,1)}, bf16[512,512]{1,0:T(8,128)(2,1)}, bf16[512,512]{1,0:T(8,128)(2,1)}, bf16[512,5...) custom-call(bf16[192,512]{1,0:T(8,128)(2,1)S(1)} %get-tuple-element.16.mixed_ref, ...), custom_call_target="tpu_custom_call" | custom-call | tf_op jit(solution)/shard_map/put_out/pallas_call | solution.py:643
